TPU v7x, 32 devices: a whole 2x2x4 slice. The times are simulated.
32 devices in a mesh: ep: 32 (over z, y, x, core).
Axes of the slice: x: 2, y: 2, z: 4, core: 2. Of those that a mesh axis runs over, the one named last changes fastest.
Arguments:
- tokens: bfloat16 [512, 2048], P('ep'), may hold values from -6 to 6
- recurrent_state: float32 [512, 16, 4096], P('ep'), may hold values from -8 to 8
- first_gain: float32 [2048], replicated, may hold values from 0.1 to 1.9
- w_receptance: bfloat16 [2048, 1024], P('ep'), may hold values from -0.125 to 0.125
- w_key: bfloat16 [2048, 1024], P('ep'), may hold values from -0.125 to 0.125
- w_value: bfloat16 [2048, 1024], P('ep'), may hold values from -0.125 to 0.125
- decay_down: bfloat16 [2048, 64], replicated, may hold values from -0.125 to 0.125
- decay_up: bfloat16 [64, 1024], replicated, may hold values from -0.75 to 0.75
- decay_base: float32 [1024], replicated, may hold values from -4 to 1
- rate_down: bfloat16 [2048, 64], replicated, may hold values from -0.125 to 0.125
- rate_up: bfloat16 [64, 1024], replicated, may hold values from -0.75 to 0.75
- rate_base: float32 [1024], replicated, may hold values from -5 to 5
- key_scale: float32 [1024], replicated, may hold values from 0.25 to 4
- head_gain: float32 [1024], replicated, may hold values from 0.1 to 1.9
- w_output: bfloat16 [1024, 2048], replicated, may hold values from -0.1875 to 0.1875
- second_gain: float32 [2048], replicated, may hold values from 0.1 to 1.9
- shared_gate: bfloat16 [2048, 512], replicated, may hold values from -0.125 to 0.125
- shared_up: bfloat16 [2048, 512], replicated, may hold values from -0.125 to 0.125
- shared_down: bfloat16 [512, 2048], replicated, may hold values from -0.25 to 0.25
- expert_gate: bfloat16 [32, 2048, 512], P('ep'), may hold values from -0.125 to 0.125
- expert_up: bfloat16 [32, 2048, 512], P('ep'), may hold values from -0.125 to 0.125
- expert_down: bfloat16 [32, 512, 2048], P('ep'), may hold values from -0.25 to 0.25
- routes: int32 [512, 4], replicated, may hold values from 0 to 31, all different within a row; in each aligned block of 16 rows (0 to 15, 16 to 31, ...) at most 4 rows name the same one
- route_weights: float32 [512, 4], replicated, may hold values from 0.1 to 1
Outputs:
- new_tokens: bfloat16 [512, 2048], P('ep')
- new_state: float32 [512, 16, 4096], P('ep')
Inputs may be any that keep to these rules, and one draw needn't show every extreme that they name: `routes`: each row names 4 different experts. In the rows of one device no expert is named by more than 4 rows, a bound that some block reaches of them.
All inputs are finite; a program needn't handle non-finite values.
Results may differ from a plain program's by a relative error of at most 0.015.
Values may be sent and summed in bfloat16 or wider, within the bound.
A program may use at most 128 MiB of HBM per device.

v0:
```python
import functools

import jax
import jax.numpy as jnp
from jax import lax
from jax.experimental import pallas as pl
from jax.experimental.pallas import tpu as pltpu
from jax.sharding import PartitionSpec as P

HEAD = 64
TOPK = 4
MOST = 4
GROUP = 8
PARTS = 4
NORM_EPS = 1e-06
GROUP_EPS = 0.00064
MESH = pl.DeviceIdType.MESH
F32 = jnp.float32
BF16 = jnp.bfloat16
VMEM_BYTES = 60 * 1024 * 1024


def dot(a, b):
    return jnp.dot(a, b, preferred_element_type=F32)


def rms_scale(inputs, gain):
    widened = inputs.astype(F32)
    return (
        widened * lax.rsqrt(jnp.mean(widened * widened, axis=-1, keepdims=True) + NORM_EPS) * gain
    )


def project_kernel(
    devices,
    tokens,
    gain,
    w_r,
    w_k,
    w_v,
    decay_down,
    decay_up,
    decay_base,
    rate_down,
    rate_up,
    rate_base,
    key_scale,
    out,
    stage,
    wbuf,
    nsend,
    xbuf,
    psend,
    precv,
    local_sem,
    wsend_sem,
    wrecv_sem,
    xsend_sem,
    xrecv_sem,
    psend_sem,
    precv_sem,
):
    rows, mix = w_r.shape
    half = mix // 2
    count = tokens.shape[0]
    groups = devices // GROUP
    members = 2 * groups
    depth = tokens.shape[1] // groups
    me = lax.axis_index("ep")
    base = (me // GROUP) * GROUP
    place = me % GROUP
    core = me % 2
    column = place // 2
    member = (me // GROUP) * 2 + core
    chip = me - core
    x_bit = (place // 2) % 2
    y_bit = place // 4
    x_chip = chip + 2 - 4 * x_bit
    y_chip = chip + 4 - 8 * y_bit
    diag_chip = x_chip + 4 - 8 * y_bit
    partner = chip + 1 - core

    def peer_of(offset):
        which = (member + offset) % members
        return which, (which // 2) * GROUP + column * 2 + which % 2

    local = []
    weights = (w_r, w_k, w_v)
    for number, weight in enumerate(weights):
        for side in range(2):
            local.append(
                pltpu.make_async_copy(
                    weight.at[:, pl.ds(side * half, half)],
                    stage.at[number, side],
                    local_sem.at[number * 2 + side],
                )
            )
    for copy in local:
        copy.start()

    barrier = pltpu.get_barrier_semaphore()
    greet = [partner, x_chip, x_chip + 1, y_chip, y_chip + 1]
    greet = greet + [peer_of(offset)[1] for offset in range(1, members)]
    for peer in greet:
        pl.semaphore_signal(barrier, inc=1, device_id=(peer,), device_id_type=MESH)

    normed = rms_scale(tokens[...], gain[...]).astype(BF16)
    for number in range(groups):
        nsend[number] = normed[:, number * depth : (number + 1) * depth]
    for copy in local:
        copy.wait()
    pl.semaphore_wait(barrier, len(greet))

    def slot(number, device):
        return wbuf.at[number, pl.ds(pl.multiple_of((device - base) * rows, rows), rows), :]

    def weight_copy(number, source, landing, send, receive, target):
        return pltpu.make_async_remote_copy(
            src_ref=source,
            dst_ref=slot(number, landing),
            send_sem=wsend_sem.at[number * 7 + send],
            recv_sem=wrecv_sem.at[number * 7 + receive],
            device_id=(target,),
            device_id_type=MESH,
        )

    sends = []

    def launch(copy):
        copy.start()
        sends.append(copy)

    def direct(number):
        for side in range(2):
            source = stage.at[number, side]
            launch(weight_copy(number, source, me, 1 + side, 1 + core, x_chip + side))
            launch(weight_copy(number, source, me, 3 + side, 3 + core, y_chip + side))
        launch(weight_copy(number, stage.at[number, 1 - core], me, 0, 0, partner))

    def arrived(number, source, receive):
        weight_copy(number, stage.at[0, 0], source, 0, receive, partner).wait_recv()

    def relay(number):
        arrived(number, y_chip, 3)
        launch(weight_copy(number, slot(number, y_chip), y_chip, 5, 5, x_chip + core))
        arrived(number, x_chip + 1, 2)
        launch(weight_copy(number, slot(number, x_chip + 1), x_chip + 1, 6, 6, y_chip + core))

    direct(0)
    for offset in range(1, members):
        which, device = peer_of(offset)
        launch(
            pltpu.make_async_remote_copy(
                src_ref=nsend.at[which // 2],
                dst_ref=xbuf.at[member],
                send_sem=xsend_sem.at[offset],
                recv_sem=xrecv_sem.at[offset],
                device_id=(device,),
                device_id_type=MESH,
            )
        )
    direct(1)

    for number in range(3):
        own = stage[number, core]
        wbuf[number, pl.ds(pl.multiple_of(place * rows, rows), rows), :] = own
    xbuf[member] = nsend[me // GROUP]
    relay(0)
    direct(2)

    def put(number, values, first):
        for head in range(values.shape[1] // HEAD):
            out[number, :, first + head, :] = values[:, head * HEAD : (head + 1) * HEAD]

    heads = mix // HEAD
    flip = (((1,), (1,)), ((), ()))

    def down(matrix):
        return lax.dot_general(normed, matrix, flip, preferred_element_type=F32)

    decay_low = jnp.tanh(down(decay_down[...])).astype(BF16)
    decay_pre = decay_base[...] + dot(decay_low, decay_up[...])
    put(3, jnp.exp(-jnp.exp(-jax.nn.softplus(-decay_pre) - 0.5)), 0)
    rate_low = down(rate_down[...]).astype(BF16)
    put(4, jax.nn.sigmoid(rate_base[...] + dot(rate_low, rate_up[...])), 0)

    for offset in range(1, members):
        source = (member + members - offset) % members
        pltpu.make_async_remote_copy(
            src_ref=nsend.at[0],
            dst_ref=xbuf.at[source],
            send_sem=xsend_sem.at[offset],
            recv_sem=xrecv_sem.at[offset],
            device_id=(partner,),
            device_id_type=MESH,
        ).wait_recv()
    stacked = xbuf[...].reshape(members * count, depth)

    def part_copy(number, source, landing, offset, target):
        return pltpu.make_async_remote_copy(
            src_ref=psend.at[number, source],
            dst_ref=precv.at[number, landing],
            send_sem=psend_sem.at[number * members + offset],
            recv_sem=precv_sem.at[number * members + offset],
            device_id=(target,),
            device_id_type=MESH,
        )

    def multiply(number):
        arrived(number, partner, 0)
        arrived(number, x_chip, 1)
        arrived(number, y_chip + 1, 4)
        arrived(number, diag_chip, 5)
        arrived(number, diag_chip + 1, 6)
        part = dot(stacked, wbuf[number]).astype(BF16)
        psend[number] = part.reshape(members, count, half)
        for offset in range(1, members):
            which, device = peer_of(offset)
            launch(part_copy(number, which, member, offset, device))
        precv[number, member] = psend[number, member]

    def finish(number):
        for offset in range(1, members):
            source = (member + members - offset) % members
            part_copy(number, 0, source, offset, partner).wait_recv()
        for side in range(2):
            total = precv[number, side].astype(F32)
            for which in range(1, groups):
                total = total + precv[number, which * 2 + side].astype(F32)
            total = total.astype(BF16).astype(F32)
            put(number, total, side * (heads // 2))
            if number == 1:
                scale = key_scale[:, side * half : (side + 1) * half]
                put(5, total * scale, side * (heads // 2))

    relay(1)
    multiply(0)
    relay(2)
    multiply(1)
    finish(0)
    multiply(2)
    finish(1)
    finish(2)
    for copy in sends:
        copy.wait_send()


def project(devices, tokens, gain, w_r, w_k, w_v, dd, du, db, rd, ru, rb, scale):
    count, width = tokens.shape
    rows, mix = w_r.shape
    groups = devices // GROUP
    members = 2 * groups
    half = mix // 2
    vmem = pl.BlockSpec(memory_space=pltpu.VMEM)
    hbm = pl.BlockSpec(memory_space=pl.ANY)
    dma = pltpu.SemaphoreType.DMA
    return pl.pallas_call(
        functools.partial(project_kernel, devices),
        out_shape=jax.ShapeDtypeStruct((6, count, mix // HEAD, HEAD), F32),
        in_specs=[vmem, vmem, hbm, hbm, hbm] + [vmem] * 7,
        out_specs=vmem,
        scratch_shapes=[
            pltpu.VMEM((3, 2, rows, half), BF16),
            pltpu.VMEM((3, GROUP * rows, half), BF16),
            pltpu.VMEM((groups, count, width // groups), BF16),
            pltpu.VMEM((members, count, width // groups), BF16),
            pltpu.VMEM((3, members, count, half), BF16),
            pltpu.VMEM((3, members, count, half), BF16),
            dma((6,)),
            dma((21,)),
            dma((21,)),
            dma((members,)),
            dma((members,)),
            dma((3 * members,)),
            dma((3 * members,)),
        ],
        compiler_params=pltpu.CompilerParams(
            collective_id=0, has_side_effects=True, vmem_limit_bytes=VMEM_BYTES
        ),
        name="project",
    )(tokens, gain, w_r, w_k, w_v, dd, du, db, rd, ru, rb, scale)


def split_sum(values, ones):
    high = values.astype(BF16)
    low = (values - high.astype(F32)).astype(BF16)
    return dot(high, ones) + dot(low, ones)


def mixer_kernel(
    steps,
    vectors,
    state,
    head_gain,
    tokens,
    w_output,
    second_gain,
    new_state,
    residual,
    second,
    wbuf,
    mixed,
    sem,
):
    step = pl.program_id(0)
    _, per_step, heads, _ = vectors.shape
    entries = state.shape[2]
    span = 256
    tiles = entries // span
    copies = span // HEAD
    copy = pltpu.make_async_copy(w_output, wbuf, sem)

    @pl.when(step == 0)
    def _():
        copy.start()

    row = lax.broadcasted_iota(jnp.int32, (span, span), 0)
    col = lax.broadcasted_iota(jnp.int32, (span, span), 1)
    ones = (row // HEAD == col // HEAD).astype(F32).astype(BF16)
    lane = lax.broadcasted_iota(jnp.int32, (heads, span), 1)

    def widen(inputs):
        return jnp.concatenate([inputs] * copies, axis=1)

    for number in range(per_step):
        reader, keys, values, decay, learn, scaled = [vectors[w, number] for w in range(6)]
        direction = scaled / jnp.sqrt(jnp.sum(scaled * scaled, axis=-1, keepdims=True) + 1.0)
        wide_direction = widen(direction)
        wide_decay = widen(decay)
        wide_learn = widen(direction * learn)
        wide_keys = widen(keys)
        wide_reader = widen(reader)
        wide_values = widen(values)
        blocks = [state[number, :, i * span : (i + 1) * span] for i in range(tiles)]
        picks = [(lane % HEAD) == i * copies + lane // HEAD for i in range(tiles)]
        removed = dot(
            jnp.concatenate([(b * wide_direction).astype(BF16) for b in blocks], 0), ones
        )
        spread_values = dot(
            jnp.concatenate([jnp.where(p, wide_values, 0.0) for p in picks], 0).astype(BF16), ones
        )
        later = []
        for i in range(tiles):
            part = slice(i * heads, (i + 1) * heads)
            fresh = (
                blocks[i] * wide_decay
                - removed[part] * wide_learn
                + spread_values[part] * wide_keys
            )
            new_state[number, :, i * span : (i + 1) * span] = fresh
            later.append(fresh * wide_reader)
        read = split_sum(jnp.concatenate(later, 0), ones)
        gathered = jnp.where(picks[0], read[:heads], 0.0)
        for i in range(1, tiles):
            gathered = gathered + jnp.where(picks[i], read[i * heads : (i + 1) * heads], 0.0)
        readout = gathered[:, :HEAD]
        for i in range(1, copies):
            readout = readout + gathered[:, i * HEAD : (i + 1) * HEAD]
        centre = jnp.mean(readout, axis=-1, keepdims=True)
        spread = jnp.mean(jnp.square(readout - centre), axis=-1, keepdims=True)
        mixed[step * per_step + number] = (
            readout - centre
        ) * lax.rsqrt(spread + GROUP_EPS)

    @pl.when(step == steps - 1)
    def _():
        count = mixed.shape[0]
        channels = heads * HEAD
        flat = mixed[...].reshape(count * heads, HEAD)
        source = lax.broadcasted_iota(jnp.int32, (HEAD, channels), 0)
        target = lax.broadcasted_iota(jnp.int32, (HEAD, channels), 1)
        tiled = split_sum(flat, (target % HEAD == source).astype(F32).astype(BF16))
        head = lax.broadcasted_iota(jnp.int32, (count * heads, channels), 0) % heads
        channel = lax.broadcasted_iota(jnp.int32, (count * heads, channels), 1) // HEAD
        kept = (jnp.where(head == channel, tiled, 0.0) * head_gain[...]).astype(BF16)
        owner = lax.broadcasted_iota(jnp.int32, (count, count * heads), 1) // heads
        token = lax.broadcasted_iota(jnp.int32, (count, count * heads), 0)
        rows = dot((owner == token).astype(F32).astype(BF16), kept).astype(BF16)
        copy.wait()
        after = (tokens[...].astype(F32) + dot(rows, wbuf[...])).astype(BF16)
        residual[...] = after
        second[...] = rms_scale(after, second_gain[...]).astype(BF16)


def mixer(vectors, state, head_gain, tokens, w_output, second_gain):
    _, count, heads, _ = vectors.shape
    width = tokens.shape[1]
    entries = state.shape[2]
    per_step = 2 if count % 2 == 0 else 1
    steps = count // per_step
    whole = lambda array: pl.BlockSpec(array.shape, lambda i: (0,) * array.ndim)
    block = pl.BlockSpec((per_step, heads, entries), lambda i: (i, 0, 0))
    flat = pl.BlockSpec((count, width), lambda i: (0, 0))
    return pl.pallas_call(
        functools.partial(mixer_kernel, steps),
        grid=(steps,),
        out_shape=[
            jax.ShapeDtypeStruct(state.shape, F32),
            jax.ShapeDtypeStruct((count, width), BF16),
            jax.ShapeDtypeStruct((count, width), BF16),
        ],
        in_specs=[
            pl.BlockSpec((6, per_step, heads, HEAD), lambda i: (0, i, 0, 0)),
            block,
            whole(head_gain),
            flat,
            pl.BlockSpec(memory_space=pl.ANY),
            whole(second_gain),
        ],
        out_specs=[block, flat, flat],
        scratch_shapes=[
            pltpu.VMEM(w_output.shape, BF16),
            pltpu.VMEM((count, heads, HEAD), F32),
            pltpu.SemaphoreType.DMA,
        ],
        compiler_params=pltpu.CompilerParams(
            dimension_semantics=("arbitrary",), vmem_limit_bytes=VMEM_BYTES
        ),
        name="mixer",
    )(vectors, state, head_gain, tokens, w_output, second_gain)


def onehot(flags):
    return flags.astype(F32).astype(BF16)


def onehot_values(values):
    return values.astype(F32).astype(BF16)


def thirds(values):
    first = values.astype(BF16)
    rest = values - first.astype(F32)
    middle = rest.astype(BF16)
    return first, middle, (rest - middle.astype(F32)).astype(BF16)


def experts_kernel(
    devices,
    second,
    residual,
    routes,
    route_weights,
    shared_gate,
    shared_up,
    shared_down,
    expert_gate,
    expert_up,
    expert_down,
    out,
    sg,
    su,
    sd,
    eg,
    eu,
    ed,
    sbuf,
    rbuf,
    pbuf,
    abuf,
    xfull,
    local_sem,
    osend_sem,
    orecv_sem,
    bsend_sem,
    brecv_sem,
):
    count, width = second.shape
    part = width // PARTS
    block = PARTS * MOST
    total = devices * block
    tall = PARTS * count
    me = lax.axis_index("ep")
    barrier = pltpu.get_barrier_semaphore()

    def greet(offset, carry):
        pl.semaphore_signal(
            barrier, inc=1, device_id=((me + offset) % devices,), device_id_type=MESH
        )
        return carry

    lax.fori_loop(1, devices, greet, 0)
    loads = [
        pltpu.make_async_copy(source, target, local_sem.at[number])
        for number, (source, target) in enumerate(
            (
                (shared_gate, sg),
                (shared_up, su),
                (expert_gate.at[0], eg),
                (expert_up.at[0], eu),
                (shared_down, sd),
                (expert_down.at[0], ed),
            )
        )
    ]
    for load in loads:
        load.start()

    rows = second[...]
    lines = lax.broadcasted_iota(jnp.int32, (routes.shape[1], PARTS * count), 0)
    lanes = lax.broadcasted_iota(jnp.int32, (routes.shape[1], PARTS * count), 1)
    pick = onehot(lines == me * count + lanes % count)
    routes_wide = dot(onehot_values(routes[...]), pick)
    stacked = jnp.concatenate([rows[:, q * part : (q + 1) * part] for q in range(PARTS)], 0)
    line = lax.broadcasted_iota(jnp.int32, (total, tall), 0)
    lane = lax.broadcasted_iota(jnp.int32, (total, tall), 1)
    named = line < 0
    for j in range(TOPK):
        named = named | (routes_wide[j : j + 1, :] == (line // block).astype(F32))
    up_row = lax.broadcasted_iota(jnp.int32, (tall, tall), 0)
    up_col = lax.broadcasted_iota(jnp.int32, (tall, tall), 1)
    same = up_row // count == up_col // count
    before = dot(onehot(named), onehot(same & (up_row < up_col)))
    fits = (before == (line % MOST).astype(F32)) & (lane // count == (line % block) // MOST)
    outgoing = dot(onehot(named & fits), stacked).astype(BF16)
    sbuf[...] = outgoing.reshape(devices, block, part)
    pl.semaphore_wait(barrier, devices - 1)

    def exchange(source_ref, target_ref, send, receive, offset, landing):
        peer = (me + offset) % devices
        return pltpu.make_async_remote_copy(
            src_ref=source_ref.at[peer],
            dst_ref=target_ref.at[landing],
            send_sem=send.at[offset],
            recv_sem=receive.at[offset],
            device_id=(peer,),
            device_id_type=MESH,
        )

    def start_all(source_ref, target_ref, send, receive):
        def one(turn, carry):
            offset = devices // 2 + (1 - 2 * (turn % 2)) * ((turn + 1) // 2)
            exchange(source_ref, target_ref, send, receive, offset, me).start()
            return carry

        lax.fori_loop(0, devices - 1, one, 0)

    def receive_all(source_ref, target_ref, send, receive):
        def one(offset, carry):
            origin = (me + devices - offset) % devices
            exchange(source_ref, target_ref, send, receive, offset, origin).wait_recv()
            return carry

        lax.fori_loop(1, devices, one, 0)

    def sent_all(source_ref, target_ref, send, receive):
        def one(offset, carry):
            exchange(source_ref, target_ref, send, receive, offset, me).wait_send()
            return carry

        lax.fori_loop(1, devices, one, 0)

    there = (sbuf, rbuf, osend_sem, orecv_sem)
    back = (pbuf, abuf, bsend_sem, brecv_sem)
    start_all(*there)
    rbuf[me] = sbuf[me]

    def gated(inputs, gate_ref, up_ref):
        gate_part = dot(inputs, gate_ref[...])
        up_part = dot(inputs, up_ref[...])
        return (jax.nn.silu(gate_part) * up_part).astype(BF16)

    loads[0].wait()
    loads[1].wait()
    shared_hidden = gated(rows, sg, su)
    loads[4].wait()
    shared = dot(shared_hidden, sd[...])

    across = lax.broadcasted_iota(jnp.int32, (tall, total), 1)
    down = lax.broadcasted_iota(jnp.int32, (tall, total), 0)
    named_t = across < 0
    turned = (((1,), (1,)), ((), ()))
    lines_t = lax.broadcasted_iota(jnp.int32, (tall, routes.shape[1]), 1)
    lanes_t = lax.broadcasted_iota(jnp.int32, (tall, routes.shape[1]), 0)
    pick_t = onehot(lines_t == me * count + lanes_t % count)

    def picked(values):
        return lax.dot_general(pick_t, values, turned, preferred_element_type=F32)

    routes_tall = picked(onehot_values(routes[...]))
    weights_tall = sum(picked(piece) for piece in thirds(route_weights[...]))
    weight_t = jnp.zeros((tall, total), F32)
    for j in range(TOPK):
        hit = routes_tall[:, j : j + 1] == (across // block).astype(F32)
        named_t = named_t | hit
        weight_t = weight_t + jnp.where(hit, weights_tall[:, j : j + 1], 0.0)
    before_t = dot(onehot(same & (up_col < up_row)), onehot(named_t))
    fits_t = (before_t == (across % MOST).astype(F32)) & (
        down // count == (across % block) // MOST
    )
    weight_t = jnp.where(fits_t, weight_t, 0.0)
    first, middle, last = thirds(weight_t)

    slots = devices * MOST
    narrow = lax.broadcasted_iota(jnp.int32, (slots, total), 0)
    broad = lax.broadcasted_iota(jnp.int32, (slots, total), 1)
    tall_row = lax.broadcasted_iota(jnp.int32, (total, slots), 0)
    tall_col = lax.broadcasted_iota(jnp.int32, (total, slots), 1)
    takes = []
    gives = []
    for q in range(PARTS):
        takes.append(onehot(broad == narrow // MOST * block + q * MOST + narrow % MOST))
        gives.append(onehot(tall_row == tall_col // MOST * block + q * MOST + tall_col % MOST))

    receive_all(*there)
    received = rbuf[...].reshape(total, part)
    for q in range(PARTS):
        xfull[:, q * part : (q + 1) * part] = dot(takes[q], received).astype(BF16)
    loads[2].wait()
    loads[3].wait()
    hidden = gated(xfull[...], eg, eu)
    loads[5].wait()
    produced = jnp.zeros((total, part), F32)
    for q in range(PARTS):
        result = dot(hidden, ed[:, q * part : (q + 1) * part]).astype(BF16)
        produced = produced + dot(gives[q], result)
    pbuf[...] = produced.astype(BF16).reshape(devices, block, part)
    start_all(*back)
    abuf[me] = pbuf[me]
    receive_all(*back)
    answers = abuf[...].reshape(total, part)
    routed = dot(first, answers) + dot(middle, answers) + dot(last, answers)
    kept = residual[...].astype(F32) + shared
    for q in range(PARTS):
        cut = slice(q * part, (q + 1) * part)
        out[:, cut] = (kept[:, cut] + routed[q * count : (q + 1) * count]).astype(BF16)
    sent_all(*there)
    sent_all(*back)


def experts(devices, second, residual, routes, weights, *matrices):
    count, width = second.shape
    vmem = pl.BlockSpec(memory_space=pltpu.VMEM)
    hbm = pl.BlockSpec(memory_space=pl.ANY)
    dma = pltpu.SemaphoreType.DMA
    exchange = pltpu.VMEM((devices, PARTS * MOST, width // PARTS), BF16)
    return pl.pallas_call(
        functools.partial(experts_kernel, devices),
        out_shape=jax.ShapeDtypeStruct((count, width), BF16),
        in_specs=[vmem] * 4 + [hbm] * 6,
        out_specs=vmem,
        scratch_shapes=[pltpu.VMEM(m.shape[-2:], BF16) for m in matrices]
        + [exchange] * 4
        + [
            pltpu.VMEM((devices * MOST, width), BF16),
            dma((6,)),
            dma((devices,)),
            dma((devices,)),
            dma((devices,)),
            dma((devices,)),
        ],
        compiler_params=pltpu.CompilerParams(
            collective_id=1, has_side_effects=True, vmem_limit_bytes=VMEM_BYTES
        ),
        name="experts",
    )(second, residual, routes, weights, *matrices)


def per_device(
    tokens,
    recurrent_state,
    first_gain,
    w_receptance,
    w_key,
    w_value,
    decay_down,
    decay_up,
    decay_base,
    rate_down,
    rate_up,
    rate_base,
    key_scale,
    head_gain,
    w_output,
    second_gain,
    shared_gate,
    shared_up,
    shared_down,
    expert_gate,
    expert_up,
    expert_down,
    routes,
    route_weights,
):
    devices = lax.axis_size("ep")
    vectors = project(
        devices,
        tokens,
        first_gain[None, :],
        w_receptance,
        w_key,
        w_value,
        decay_down.T,
        decay_up,
        decay_base[None, :],
        rate_down.T,
        rate_up,
        rate_base[None, :],
        key_scale[None, :],
    )
    new_state, residual, second = mixer(
        vectors,
        recurrent_state,
        head_gain[None, :],
        tokens,
        w_output,
        second_gain[None, :],
    )
    new_tokens = experts(
        devices,
        second,
        residual,
        routes.T,
        route_weights.T,
        shared_gate,
        shared_up,
        shared_down,
        expert_gate,
        expert_up,
        expert_down,
    )
    return (new_tokens, new_state)


def solution(mesh):
    in_specs = (
        P("ep", None),
        P("ep", None, None),
        P(),
        P("ep", None),
        P("ep", None),
        P("ep", None),
        P(),
        P(),
        P(),
        P(),
        P(),
        P(),
        P(),
        P(),
        P(),
        P(),
        P(),
        P(),
        P(),
        P("ep", None, None),
        P("ep", None, None),
        P("ep", None, None),
        P(),
        P(),
    )
    out_specs = (P("ep", None), P("ep", None, None))
    return jax.shard_map(
        per_device, mesh=mesh, in_specs=in_specs, out_specs=out_specs, check_vma=False
    )
```

profile of v0, /device:TPU:0, one launch (start us, length us, event | category | flops | bytes accessed | tf_op | source)
XLA Modules:
  0.0 79.4 jit_solution(8657410879474210350)
XLA Ops:
  0.6 28.9 %project.1.vectors = f32[6,16,16,64]{3,2,1,0:T(8,128)} custom-call(bf16[16,2048]{1,0:T(8,128)(2,1)} %tokens.3, f32[1,2048]{1,0:T(1,128)} %bitcast.12, bf16[64,1024]{1,0:T(8,128)(2,1)} %w_r.1, bf16[64,1024]{1,0:T(8,128)(2,1)} %w_k.1, bf16[64,1024]{1,0:T(8,128)(2,1)} %w_v.1, bf16[64,2048]{1,0:T(8,128)(2,1)} %bitcast.10, bf16[64,1024]{1,0:T(8,128)(2,1)} %decay_up.1, ...), custom_call_target="tpu_custom_call" | custom-call | tf_op jit(solution)/shard_map/project/pallas_call | solution.py:257
  29.5 12.6 %mixer.1 = (f32[16,16,4096]{2,1,0:T(8,128)}, bf16[16,2048]{1,0:T(8,128)(2,1)}, bf16[16,2048]{1,0:T(8,128)(2,1)}) custom-call(f32[6,16,16,64]{3,2,1,0:T(8,128)} %project.1.vectors, f32[16,16,4096]{2,1,0:T(8,128)} %state.1, f32[1,1024]{1,0:T(1,128)} %bitcast.16, bf16[16,2048]{1,0:T(8,128)(2,1)} %tokens.3, bf16[1024,2048]{1,0:T(8,128)(2,1)} %w_output.1, ...), custom_call_target="tpu_custom_call" | custom-call | tf_op jit(solution)/shard_map/mixer/pallas_call | solution.py:394
  42.1 35.8 %experts.1 = bf16[16,2048]{1,0:T(8,128)(2,1)} custom-call(bf16[16,2048]{1,0:T(8,128)(2,1)} %get-tuple-element.5.second, bf16[16,2048]{1,0:T(8,128)(2,1)} %get-tuple-element.6.residual, s32[4,512]{1,0:T(4,128)} %bitcast.14, f32[4,512]{1,0:T(4,128)} %bitcast.15, bf16[2048,512]{1,0:T(8,128)(2,1)} %shared_gate.1, bf16[2048,512]{1,0:T(8,128)(2,1)} %shared_up.1, ...), custom_call_target="tpu_custom_call" | custom-call | tf_op jit(solution)/shard_map/experts/pallas_call | solution.py:637
  77.9 1.5 %copy.27 = bf16[16,2048]{1,0:T(8,128)(2,1)} copy(bf16[16,2048]{1,0:T(8,128)(2,1)} %experts.1) | data formatting | bytes 131072
where the time goes:
time: 79.8 us; the launch traced here: 79.4 us
  Pallas kernels  77.3 us (97%)
  local copies, waits for them, and re-layouts  1.47 us (2%)
    pallas_call x1, Pallas kernels, experts(): pl.pallas_call(functools.partial(experts_kernel, devices), out_shape=jax....  35.8 us
    pallas_call x1, Pallas kernels, project(): pl.pallas_call(functools.partial(project_kernel, devices), out_shape=jax....  28.9 us
    pallas_call x1, Pallas kernels, mixer(): pl.pallas_call(functools.partial(mixer_kernel, steps), grid=(steps,), out...  12.6 us

commit v1 on v0

--- a/solution.py
+++ b/solution.py
@@ -12,6 +12,7 @@
 MOST = 4
 GROUP = 8
 PARTS = 4
+SPAN = 256
 NORM_EPS = 1e-06
 GROUP_EPS = 0.00064
 MESH = pl.DeviceIdType.MESH
@@ -288,9 +289,8 @@
 
 
 def mixer_kernel(
-    steps,
-    vectors,
-    state,
+    vectors_in,
+    state_in,
     head_gain,
     tokens,
     w_output,
@@ -298,21 +298,40 @@
     new_state,
     residual,
     second,
+    vectors,
+    state,
+    fresh_out,
     wbuf,
     mixed,
-    sem,
+    work,
+    sums,
+    vec_sem,
+    in_sem,
+    out_sem,
+    w_sem,
 ):
-    step = pl.program_id(0)
-    _, per_step, heads, _ = vectors.shape
+    _, count, heads, _ = vectors.shape
     entries = state.shape[2]
-    span = 256
+    steps = in_sem.shape[0]
+    per_step = count // steps
+    span = SPAN
     tiles = entries // span
     copies = span // HEAD
-    copy = pltpu.make_async_copy(w_output, wbuf, sem)
-
-    @pl.when(step == 0)
-    def _():
-        copy.start()
+
+    def rows_of(step):
+        return pl.ds(step * per_step, per_step)
+
+    def state_load(step):
+        return pltpu.make_async_copy(
+            state_in.at[rows_of(step)], state.at[rows_of(step)], in_sem.at[step]
+        )
+
+    vector_load = pltpu.make_async_copy(vectors_in, vectors, vec_sem)
+    weight_load = pltpu.make_async_copy(w_output, wbuf, w_sem)
+    vector_load.start()
+    for step in range(steps):
+        state_load(step).start()
+    weight_load.start()
 
     row = lax.broadcasted_iota(jnp.int32, (span, span), 0)
     col = lax.broadcasted_iota(jnp.int32, (span, span), 1)
@@ -322,100 +341,120 @@
     def widen(inputs):
         return jnp.concatenate([inputs] * copies, axis=1)
 
-    for number in range(per_step):
-        reader, keys, values, decay, learn, scaled = [vectors[w, number] for w in range(6)]
-        direction = scaled / jnp.sqrt(jnp.sum(scaled * scaled, axis=-1, keepdims=True) + 1.0)
-        wide_direction = widen(direction)
-        wide_decay = widen(decay)
-        wide_learn = widen(direction * learn)
-        wide_keys = widen(keys)
-        wide_reader = widen(reader)
-        wide_values = widen(values)
-        blocks = [state[number, :, i * span : (i + 1) * span] for i in range(tiles)]
-        picks = [(lane % HEAD) == i * copies + lane // HEAD for i in range(tiles)]
-        removed = dot(
-            jnp.concatenate([(b * wide_direction).astype(BF16) for b in blocks], 0), ones
-        )
-        spread_values = dot(
-            jnp.concatenate([jnp.where(p, wide_values, 0.0) for p in picks], 0).astype(BF16), ones
-        )
-        later = []
-        for i in range(tiles):
-            part = slice(i * heads, (i + 1) * heads)
-            fresh = (
-                blocks[i] * wide_decay
-                - removed[part] * wide_learn
-                + spread_values[part] * wide_keys
+    vector_load.wait()
+
+    def one_step(step, carry):
+        state_load(step).wait()
+        size = tiles * heads
+        kept = []
+        for place in range(per_step):
+            number = step * per_step + place
+            reader, keys, values, decay, learn, scaled = [vectors[w, number] for w in range(6)]
+            direction = scaled / jnp.sqrt(jnp.sum(scaled * scaled, axis=-1, keepdims=True) + 1.0)
+            learned = direction * learn
+            wide_direction = widen(direction)
+            wide_values = widen(values)
+            wide_reader = widen(reader * decay)
+            base = place * 3 * size
+            for i in range(tiles):
+                block = state[number, :, i * span : (i + 1) * span]
+                pick = lane % HEAD == i * copies + lane // HEAD
+                part = slice(base + i * heads, base + (i + 1) * heads)
+                work[part] = (block * wide_direction).astype(BF16)
+                part = slice(base + size + i * heads, base + size + (i + 1) * heads)
+                work[part] = jnp.where(pick, wide_values, 0.0).astype(BF16)
+                product = block * wide_reader
+                high = product.astype(BF16)
+                part = slice(base + 2 * size + i * heads, base + 2 * size + (i + 1) * heads)
+                work[part] = high
+            along_learned = jnp.sum(learned * reader, axis=-1, keepdims=True)
+            along_keys = jnp.sum(keys * reader, axis=-1, keepdims=True)
+            kept.append(
+                (number, base, widen(decay), widen(learned), widen(keys))
+                + (along_learned, along_keys, values)
             )
-            new_state[number, :, i * span : (i + 1) * span] = fresh
-            later.append(fresh * wide_reader)
-        read = split_sum(jnp.concatenate(later, 0), ones)
-        gathered = jnp.where(picks[0], read[:heads], 0.0)
-        for i in range(1, tiles):
-            gathered = gathered + jnp.where(picks[i], read[i * heads : (i + 1) * heads], 0.0)
-        readout = gathered[:, :HEAD]
-        for i in range(1, copies):
-            readout = readout + gathered[:, i * HEAD : (i + 1) * HEAD]
-        centre = jnp.mean(readout, axis=-1, keepdims=True)
-        spread = jnp.mean(jnp.square(readout - centre), axis=-1, keepdims=True)
-        mixed[step * per_step + number] = (
-            readout - centre
-        ) * lax.rsqrt(spread + GROUP_EPS)
-
-    @pl.when(step == steps - 1)
-    def _():
-        count = mixed.shape[0]
-        channels = heads * HEAD
-        flat = mixed[...].reshape(count * heads, HEAD)
-        source = lax.broadcasted_iota(jnp.int32, (HEAD, channels), 0)
-        target = lax.broadcasted_iota(jnp.int32, (HEAD, channels), 1)
-        tiled = split_sum(flat, (target % HEAD == source).astype(F32).astype(BF16))
-        head = lax.broadcasted_iota(jnp.int32, (count * heads, channels), 0) % heads
-        channel = lax.broadcasted_iota(jnp.int32, (count * heads, channels), 1) // HEAD
-        kept = (jnp.where(head == channel, tiled, 0.0) * head_gain[...]).astype(BF16)
-        owner = lax.broadcasted_iota(jnp.int32, (count, count * heads), 1) // heads
-        token = lax.broadcasted_iota(jnp.int32, (count, count * heads), 0)
-        rows = dot((owner == token).astype(F32).astype(BF16), kept).astype(BF16)
-        copy.wait()
-        after = (tokens[...].astype(F32) + dot(rows, wbuf[...])).astype(BF16)
-        residual[...] = after
-        second[...] = rms_scale(after, second_gain[...]).astype(BF16)
+        sums[...] = dot(work[...], ones)
+        for number, base, wide_decay, wide_learn, wide_keys, along_learned, along_keys, values in kept:
+            picked_removed = jnp.zeros((heads, span), F32)
+            picked_read = jnp.zeros((heads, span), F32)
+            for i in range(tiles):
+                block = state[number, :, i * span : (i + 1) * span]
+                pick = lane % HEAD == i * copies + lane // HEAD
+
+                def summed(which):
+                    first = base + which * size + i * heads
+                    return sums[first : first + heads]
+
+                removed = summed(0)
+                fresh_out[number, :, i * span : (i + 1) * span] = (
+                    block * wide_decay - removed * wide_learn + summed(1) * wide_keys
+                )
+                picked_removed = jnp.where(pick, removed, picked_removed)
+                picked_read = jnp.where(pick, summed(2), picked_read)
+            picked = picked_read - picked_removed * along_learned
+            readout = values * along_keys
+            for i in range(copies):
+                readout = readout + picked[:, i * HEAD : (i + 1) * HEAD]
+            centre = jnp.mean(readout, axis=-1, keepdims=True)
+            spread = jnp.mean(jnp.square(readout - centre), axis=-1, keepdims=True)
+            mixed[number] = (readout - centre) * lax.rsqrt(spread + GROUP_EPS)
+        pltpu.make_async_copy(
+            fresh_out.at[rows_of(step)], new_state.at[rows_of(step)], out_sem
+        ).start()
+        return carry
+
+    lax.fori_loop(0, steps, one_step, 0)
+
+    channels = heads * HEAD
+    flat = mixed[...].reshape(count * heads, HEAD)
+    source = lax.broadcasted_iota(jnp.int32, (HEAD, channels), 0)
+    target = lax.broadcasted_iota(jnp.int32, (HEAD, channels), 1)
+    tiled = split_sum(flat, (target % HEAD == source).astype(F32).astype(BF16))
+    head = lax.broadcasted_iota(jnp.int32, (count * heads, channels), 0) % heads
+    channel = lax.broadcasted_iota(jnp.int32, (count * heads, channels), 1) // HEAD
+    kept = (jnp.where(head == channel, tiled, 0.0) * head_gain[...]).astype(BF16)
+    owner = lax.broadcasted_iota(jnp.int32, (count, count * heads), 1) // heads
+    token = lax.broadcasted_iota(jnp.int32, (count, count * heads), 0)
+    rows = dot((owner == token).astype(F32).astype(BF16), kept).astype(BF16)
+    weight_load.wait()
+    after = (tokens[...].astype(F32) + dot(rows, wbuf[...])).astype(BF16)
+    residual[...] = after
+    second[...] = rms_scale(after, second_gain[...]).astype(BF16)
+    pltpu.make_async_copy(fresh_out, new_state, out_sem).wait()
 
 
 def mixer(vectors, state, head_gain, tokens, w_output, second_gain):
     _, count, heads, _ = vectors.shape
     width = tokens.shape[1]
-    entries = state.shape[2]
-    per_step = 2 if count % 2 == 0 else 1
+    per_step = 8 if count % 8 == 0 else 1
     steps = count // per_step
-    whole = lambda array: pl.BlockSpec(array.shape, lambda i: (0,) * array.ndim)
-    block = pl.BlockSpec((per_step, heads, entries), lambda i: (i, 0, 0))
-    flat = pl.BlockSpec((count, width), lambda i: (0, 0))
+    rows = per_step * 3 * state.shape[1] * (state.shape[2] // SPAN)
+    vmem = pl.BlockSpec(memory_space=pltpu.VMEM)
+    hbm = pl.BlockSpec(memory_space=pl.ANY)
+    dma = pltpu.SemaphoreType.DMA
     return pl.pallas_call(
-        functools.partial(mixer_kernel, steps),
-        grid=(steps,),
+        mixer_kernel,
         out_shape=[
             jax.ShapeDtypeStruct(state.shape, F32),
             jax.ShapeDtypeStruct((count, width), BF16),
             jax.ShapeDtypeStruct((count, width), BF16),
         ],
-        in_specs=[
-            pl.BlockSpec((6, per_step, heads, HEAD), lambda i: (0, i, 0, 0)),
-            block,
-            whole(head_gain),
-            flat,
-            pl.BlockSpec(memory_space=pl.ANY),
-            whole(second_gain),
-        ],
-        out_specs=[block, flat, flat],
+        in_specs=[hbm, hbm, vmem, vmem, hbm, vmem],
+        out_specs=[hbm, vmem, vmem],
         scratch_shapes=[
+            pltpu.VMEM(vectors.shape, F32),
+            pltpu.VMEM(state.shape, F32),
+            pltpu.VMEM(state.shape, F32),
             pltpu.VMEM(w_output.shape, BF16),
             pltpu.VMEM((count, heads, HEAD), F32),
-            pltpu.SemaphoreType.DMA,
+            pltpu.VMEM((rows, SPAN), BF16),
+            pltpu.VMEM((rows, SPAN), F32),
+            dma,
+            dma((steps,)),
+            dma,
+            dma,
         ],
-        compiler_params=pltpu.CompilerParams(
-            dimension_semantics=("arbitrary",), vmem_limit_bytes=VMEM_BYTES
-        ),
+        compiler_params=pltpu.CompilerParams(vmem_limit_bytes=VMEM_BYTES),
         name="mixer",
     )(vectors, state, head_gain, tokens, w_output, second_gain)
 

time: 79.8 us -> 75.6 us (0.947)
  Pallas kernels: 77.3 us -> 73.1 us
    pallas_call x1, Pallas kernels: 12.6 us -> 8.4 us  [mixer(): pl.pallas_call(mixer_kernel, out_shape=[jax.ShapeDtypeStruct(state.shape,...]
where the time goes in v1:
time: 75.6 us; the launch traced here: 75.2 us
  Pallas kernels  73.1 us (97%)
  local copies, waits for them, and re-layouts  1.47 us (2%)
    pallas_call x1, Pallas kernels, experts(): pl.pallas_call(functools.partial(experts_kernel, devices), out_shape=jax....  35.8 us
    pallas_call x1, Pallas kernels, project(): pl.pallas_call(functools.partial(project_kernel, devices), out_shape=jax....  28.9 us
    pallas_call x1, Pallas kernels, mixer(): pl.pallas_call(mixer_kernel, out_shape=[jax.ShapeDtypeStruct(state.shape,...  8.4 us

profile of v1, /device:TPU:0, one launch (start us, length us, event | category | flops | bytes accessed | tf_op | source)
XLA Modules:
  0.0 75.2 jit_solution(13384520398908913652)
XLA Ops:
  0.6 28.9 %project.1.vectors_in = f32[6,16,16,64]{3,2,1,0:T(8,128)} custom-call(bf16[16,2048]{1,0:T(8,128)(2,1)} %tokens.3, f32[1,2048]{1,0:T(1,128)} %bitcast.12, bf16[64,1024]{1,0:T(8,128)(2,1)} %w_r.1, bf16[64,1024]{1,0:T(8,128)(2,1)} %w_k.1, bf16[64,1024]{1,0:T(8,128)(2,1)} %w_v.1, bf16[64,2048]{1,0:T(8,128)(2,1)} %bitcast.10, bf16[64,1024]{1,0:T(8,128)(2,1)} %decay_up.1, ...), custom_call_target="tpu_custom_call" | custom-call | tf_op jit(solution)/shard_map/project/pallas_call | solution.py:258
  29.5 8.4 %mixer.1 = (f32[16,16,4096]{2,1,0:T(8,128)}, bf16[16,2048]{1,0:T(8,128)(2,1)}, bf16[16,2048]{1,0:T(8,128)(2,1)}) custom-call(f32[6,16,16,64]{3,2,1,0:T(8,128)} %project.1.vectors_in, f32[16,16,4096]{2,1,0:T(8,128)} %state_in.1, f32[1,1024]{1,0:T(1,128)} %bitcast.16, bf16[16,2048]{1,0:T(8,128)(2,1)} %tokens.3, bf16[1024,2048]{1,0:T(8,128)(2,1)} %w_output.1, ...), custom_call_target="tpu_custom_call" | custom-call | tf_op jit(solution)/shard_map/mixer/pallas_call | solution.py:435
  37.9 35.8 %experts.1 = bf16[16,2048]{1,0:T(8,128)(2,1)} custom-call(bf16[16,2048]{1,0:T(8,128)(2,1)} %get-tuple-element.5.second, bf16[16,2048]{1,0:T(8,128)(2,1)} %get-tuple-element.6.residual, s32[4,512]{1,0:T(4,128)} %bitcast.14, f32[4,512]{1,0:T(4,128)} %bitcast.15, bf16[2048,512]{1,0:T(8,128)(2,1)} %shared_gate.1, bf16[2048,512]{1,0:T(8,128)(2,1)} %shared_up.1, ...), custom_call_target="tpu_custom_call" | custom-call | tf_op jit(solution)/shard_map/experts/pallas_call | solution.py:676
  73.8 1.5 %copy.27 = bf16[16,2048]{1,0:T(8,128)(2,1)} copy(bf16[16,2048]{1,0:T(8,128)(2,1)} %experts.1) | data formatting | bytes 131072

commit v2 on v1

--- a/solution.py
+++ b/solution.py
@@ -13,6 +13,7 @@
 GROUP = 8
 PARTS = 4
 SPAN = 256
+SPLIT = 2
 NORM_EPS = 1e-06
 GROUP_EPS = 0.00064
 MESH = pl.DeviceIdType.MESH
@@ -34,11 +35,21 @@
 
 def project_kernel(
     devices,
-    tokens,
-    gain,
+    tokens_in,
+    gain_in,
+    decay_down_in,
+    decay_up_in,
+    decay_base_in,
+    rate_down_in,
+    rate_up_in,
+    rate_base_in,
+    key_scale_in,
     w_r,
     w_k,
     w_v,
+    out,
+    tokens,
+    gain,
     decay_down,
     decay_up,
     decay_base,
@@ -46,13 +57,13 @@
     rate_up,
     rate_base,
     key_scale,
-    out,
     stage,
     wbuf,
     nsend,
     xbuf,
     psend,
     precv,
+    small_sem,
     local_sem,
     wsend_sem,
     wrecv_sem,
@@ -63,6 +74,8 @@
 ):
     rows, mix = w_r.shape
     half = mix // 2
+    piece = half // SPLIT
+    pieces = 3 * SPLIT
     count = tokens.shape[0]
     groups = devices // GROUP
     members = 2 * groups
@@ -85,89 +98,109 @@
         which = (member + offset) % members
         return which, (which // 2) * GROUP + column * 2 + which % 2
 
-    local = []
-    weights = (w_r, w_k, w_v)
-    for number, weight in enumerate(weights):
-        for side in range(2):
-            local.append(
-                pltpu.make_async_copy(
-                    weight.at[:, pl.ds(side * half, half)],
-                    stage.at[number, side],
-                    local_sem.at[number * 2 + side],
-                )
-            )
-    for copy in local:
-        copy.start()
-
     barrier = pltpu.get_barrier_semaphore()
     greet = [partner, x_chip, x_chip + 1, y_chip, y_chip + 1]
     greet = greet + [peer_of(offset)[1] for offset in range(1, members)]
     for peer in greet:
         pl.semaphore_signal(barrier, inc=1, device_id=(peer,), device_id_type=MESH)
 
+    smalls = [
+        pltpu.make_async_copy(source, target, small_sem.at[number])
+        for number, (source, target) in enumerate(
+            (
+                (tokens_in, tokens),
+                (gain_in, gain),
+                (decay_down_in, decay_down),
+                (decay_up_in, decay_up),
+                (decay_base_in, decay_base),
+                (rate_down_in, rate_down),
+                (rate_up_in, rate_up),
+                (rate_base_in, rate_base),
+                (key_scale_in, key_scale),
+            )
+        )
+    ]
+    for small in smalls[:2]:
+        small.start()
+    for number, weight in enumerate((w_r, w_k, w_v)):
+        for sub in range(SPLIT):
+            for side in range(2):
+                pltpu.make_async_copy(
+                    weight.at[:, pl.ds(side * half + sub * piece, piece)],
+                    stage.at[number * SPLIT + sub, side],
+                    local_sem.at[number],
+                ).start()
+    for small in smalls[2:]:
+        small.start()
+
+    def loaded(number):
+        span = stage.at[pl.ds(number * SPLIT, SPLIT)]
+        pltpu.make_async_copy(span, span, local_sem.at[number]).wait()
+
+    for small in smalls[:2]:
+        small.wait()
     normed = rms_scale(tokens[...], gain[...]).astype(BF16)
     for number in range(groups):
         nsend[number] = normed[:, number * depth : (number + 1) * depth]
-    for copy in local:
-        copy.wait()
+    loaded(0)
     pl.semaphore_wait(barrier, len(greet))
 
     def slot(number, device):
         return wbuf.at[number, pl.ds(pl.multiple_of((device - base) * rows, rows), rows), :]
 
-    def weight_copy(number, source, landing, send, receive, target):
+    def remote(source, target, send, receive, device):
         return pltpu.make_async_remote_copy(
             src_ref=source,
-            dst_ref=slot(number, landing),
-            send_sem=wsend_sem.at[number * 7 + send],
-            recv_sem=wrecv_sem.at[number * 7 + receive],
-            device_id=(target,),
+            dst_ref=target,
+            send_sem=send,
+            recv_sem=receive,
+            device_id=(device,),
             device_id_type=MESH,
         )
 
-    sends = []
-
-    def launch(copy):
-        copy.start()
-        sends.append(copy)
+    def weight_copy(number, source, landing, kind, target):
+        return remote(
+            source, slot(number, landing), wsend_sem, wrecv_sem.at[number * 3 + kind], target
+        )
 
     def direct(number):
         for side in range(2):
             source = stage.at[number, side]
-            launch(weight_copy(number, source, me, 1 + side, 1 + core, x_chip + side))
-            launch(weight_copy(number, source, me, 3 + side, 3 + core, y_chip + side))
-        launch(weight_copy(number, stage.at[number, 1 - core], me, 0, 0, partner))
-
-    def arrived(number, source, receive):
-        weight_copy(number, stage.at[0, 0], source, 0, receive, partner).wait_recv()
+            own_side = 1 - core
+            weight_copy(number, source, me, core * 2, x_chip + side).start()
+            weight_copy(number, source, me, own_side, y_chip + side).start()
+        weight_copy(number, stage.at[number, 1 - core], me, 0, partner).start()
+
+    def arrived(number, source, kind):
+        weight_copy(number, stage.at[0, 0], source, kind, partner).wait_recv()
 
     def relay(number):
-        arrived(number, y_chip, 3)
-        launch(weight_copy(number, slot(number, y_chip), y_chip, 5, 5, x_chip + core))
+        arrived(number, y_chip, 1)
+        weight_copy(number, slot(number, y_chip), y_chip, 0, x_chip + core).start()
         arrived(number, x_chip + 1, 2)
-        launch(weight_copy(number, slot(number, x_chip + 1), x_chip + 1, 6, 6, y_chip + core))
+        weight_copy(number, slot(number, x_chip + 1), x_chip + 1, 0, y_chip + core).start()
+
+    def rest(number):
+        span = wbuf.at[number, pl.ds(0, 5 * rows), :]
+        remote(span, span, wsend_sem, wrecv_sem.at[number * 3], partner).wait_recv()
+
+    def own(number):
+        mine = stage[number, core]
+        wbuf[number, pl.ds(pl.multiple_of(place * rows, rows), rows), :] = mine
 
     direct(0)
     for offset in range(1, members):
         which, device = peer_of(offset)
-        launch(
-            pltpu.make_async_remote_copy(
-                src_ref=nsend.at[which // 2],
-                dst_ref=xbuf.at[member],
-                send_sem=xsend_sem.at[offset],
-                recv_sem=xrecv_sem.at[offset],
-                device_id=(device,),
-                device_id_type=MESH,
-            )
-        )
+        remote(nsend.at[which // 2], xbuf.at[member], xsend_sem, xrecv_sem, device).start()
     direct(1)
-
-    for number in range(3):
-        own = stage[number, core]
-        wbuf[number, pl.ds(pl.multiple_of(place * rows, rows), rows), :] = own
+    loaded(1)
+    direct(2)
+    loaded(2)
+    for number in range(pieces):
+        own(number)
     xbuf[member] = nsend[me // GROUP]
     relay(0)
-    direct(2)
+    direct(3)
 
     def put(number, values, first):
         for head in range(values.shape[1] // HEAD):
@@ -179,107 +212,109 @@
     def down(matrix):
         return lax.dot_general(normed, matrix, flip, preferred_element_type=F32)
 
+    for small in smalls[2:]:
+        small.wait()
     decay_low = jnp.tanh(down(decay_down[...])).astype(BF16)
     decay_pre = decay_base[...] + dot(decay_low, decay_up[...])
     put(3, jnp.exp(-jnp.exp(-jax.nn.softplus(-decay_pre) - 0.5)), 0)
+    relay(1)
+    direct(4)
     rate_low = down(rate_down[...]).astype(BF16)
     put(4, jax.nn.sigmoid(rate_base[...] + dot(rate_low, rate_up[...])), 0)
-
-    for offset in range(1, members):
-        source = (member + members - offset) % members
-        pltpu.make_async_remote_copy(
-            src_ref=nsend.at[0],
-            dst_ref=xbuf.at[source],
-            send_sem=xsend_sem.at[offset],
-            recv_sem=xrecv_sem.at[offset],
-            device_id=(partner,),
-            device_id_type=MESH,
-        ).wait_recv()
+    relay(2)
+    direct(5)
+
+    others = pl.ds(0, members - 1)
+    remote(xbuf.at[others], xbuf.at[others], xsend_sem, xrecv_sem, partner).wait_recv()
     stacked = xbuf[...].reshape(members * count, depth)
 
-    def part_copy(number, source, landing, offset, target):
-        return pltpu.make_async_remote_copy(
-            src_ref=psend.at[number, source],
-            dst_ref=precv.at[number, landing],
-            send_sem=psend_sem.at[number * members + offset],
-            recv_sem=precv_sem.at[number * members + offset],
-            device_id=(target,),
-            device_id_type=MESH,
-        )
-
     def multiply(number):
-        arrived(number, partner, 0)
-        arrived(number, x_chip, 1)
-        arrived(number, y_chip + 1, 4)
-        arrived(number, diag_chip, 5)
-        arrived(number, diag_chip + 1, 6)
+        rest(number)
         part = dot(stacked, wbuf[number]).astype(BF16)
-        psend[number] = part.reshape(members, count, half)
+        psend[number] = part.reshape(members, count, piece)
         for offset in range(1, members):
             which, device = peer_of(offset)
-            launch(part_copy(number, which, member, offset, device))
+            remote(
+                psend.at[number, which],
+                precv.at[number, member],
+                psend_sem,
+                precv_sem.at[number],
+                device,
+            ).start()
         precv[number, member] = psend[number, member]
 
     def finish(number):
-        for offset in range(1, members):
-            source = (member + members - offset) % members
-            part_copy(number, 0, source, offset, partner).wait_recv()
+        span = precv.at[number, others]
+        remote(span, span, psend_sem, precv_sem.at[number], partner).wait_recv()
         for side in range(2):
             total = precv[number, side].astype(F32)
             for which in range(1, groups):
                 total = total + precv[number, which * 2 + side].astype(F32)
             total = total.astype(BF16).astype(F32)
-            put(number, total, side * (heads // 2))
-            if number == 1:
-                scale = key_scale[:, side * half : (side + 1) * half]
-                put(5, total * scale, side * (heads // 2))
-
-    relay(1)
+            column = side * half + number % SPLIT * piece
+            put(number // SPLIT, total, column // HEAD)
+            if number // SPLIT == 1:
+                put(5, total * key_scale[:, column : column + piece], column // HEAD)
+
     multiply(0)
-    relay(2)
+    relay(3)
     multiply(1)
+    relay(4)
+    multiply(2)
+    relay(5)
     finish(0)
-    multiply(2)
+    multiply(3)
     finish(1)
+    multiply(4)
     finish(2)
-    for copy in sends:
-        copy.wait_send()
-
-
-def project(devices, tokens, gain, w_r, w_k, w_v, dd, du, db, rd, ru, rb, scale):
-    count, width = tokens.shape
-    rows, mix = w_r.shape
+    multiply(5)
+    finish(3)
+    finish(4)
+    finish(5)
+    span = wbuf.at[:, pl.ds(0, 7 * rows), :]
+    remote(span, span, wsend_sem, wrecv_sem.at[0], partner).wait_send()
+    remote(xbuf.at[others], xbuf.at[others], xsend_sem, xrecv_sem, partner).wait_send()
+    span = psend.at[:, others]
+    remote(span, span, psend_sem, precv_sem.at[0], partner).wait_send()
+
+
+def project(devices, weights, *smalls):
+    count, width = smalls[0].shape
+    rows, mix = weights[0].shape
     groups = devices // GROUP
     members = 2 * groups
-    half = mix // 2
+    piece = mix // 2 // SPLIT
+    pieces = 3 * SPLIT
     vmem = pl.BlockSpec(memory_space=pltpu.VMEM)
     hbm = pl.BlockSpec(memory_space=pl.ANY)
     dma = pltpu.SemaphoreType.DMA
     return pl.pallas_call(
         functools.partial(project_kernel, devices),
         out_shape=jax.ShapeDtypeStruct((6, count, mix // HEAD, HEAD), F32),
-        in_specs=[vmem, vmem, hbm, hbm, hbm] + [vmem] * 7,
+        in_specs=[hbm] * 12,
         out_specs=vmem,
-        scratch_shapes=[
-            pltpu.VMEM((3, 2, rows, half), BF16),
-            pltpu.VMEM((3, GROUP * rows, half), BF16),
+        scratch_shapes=[pltpu.VMEM(array.shape, array.dtype) for array in smalls]
+        + [
+            pltpu.VMEM((pieces, 2, rows, piece), BF16),
+            pltpu.VMEM((pieces, GROUP * rows, piece), BF16),
             pltpu.VMEM((groups, count, width // groups), BF16),
             pltpu.VMEM((members, count, width // groups), BF16),
-            pltpu.VMEM((3, members, count, half), BF16),
-            pltpu.VMEM((3, members, count, half), BF16),
-            dma((6,)),
-            dma((21,)),
-            dma((21,)),
-            dma((members,)),
-            dma((members,)),
-            dma((3 * members,)),
-            dma((3 * members,)),
+            pltpu.VMEM((pieces, members, count, piece), BF16),
+            pltpu.VMEM((pieces, members, count, piece), BF16),
+            dma((9,)),
+            dma((3,)),
+            dma,
+            dma((3 * pieces,)),
+            dma,
+            dma,
+            dma,
+            dma((pieces,)),
         ],
         compiler_params=pltpu.CompilerParams(
             collective_id=0, has_side_effects=True, vmem_limit_bytes=VMEM_BYTES
         ),
         name="project",
-    )(tokens, gain, w_r, w_k, w_v, dd, du, db, rd, ru, rb, scale)
+    )(*smalls, *weights)
 
 
 def split_sum(values, ones):
@@ -476,10 +511,10 @@
 
 def experts_kernel(
     devices,
-    second,
-    residual,
-    routes,
-    route_weights,
+    second_in,
+    residual_in,
+    routes_in,
+    route_weights_in,
     shared_gate,
     shared_up,
     shared_down,
@@ -487,6 +522,10 @@
     expert_up,
     expert_down,
     out,
+    second,
+    residual,
+    routes,
+    route_weights,
     sg,
     su,
     sd,
@@ -497,37 +536,59 @@
     rbuf,
     pbuf,
     abuf,
+    hops,
     xfull,
+    small_sem,
     local_sem,
-    osend_sem,
-    orecv_sem,
-    bsend_sem,
-    brecv_sem,
+    send_sem,
+    recv_sem,
+    hop_send_sem,
+    hop_recv_sem,
 ):
     count, width = second.shape
     part = width // PARTS
     block = PARTS * MOST
     total = devices * block
     tall = PARTS * count
+    groups = devices // GROUP
+    relayed = 0
     me = lax.axis_index("ep")
+    group = me // GROUP
+    place = me % GROUP
     barrier = pltpu.get_barrier_semaphore()
-
-    def greet(offset, carry):
-        pl.semaphore_signal(
-            barrier, inc=1, device_id=((me + offset) % devices,), device_id_type=MESH
+    smalls = [
+        pltpu.make_async_copy(source, target, small_sem.at[number])
+        for number, (source, target) in enumerate(
+            (
+                (routes_in, routes),
+                (second_in, second),
+                (route_weights_in, route_weights),
+                (residual_in, residual),
+            )
         )
-        return carry
-
-    lax.fori_loop(1, devices, greet, 0)
+    ]
+    for small in smalls:
+        small.start()
+
+    def peers():
+        order = sorted(range(groups), key=lambda g: (-min(g, groups - g), g))
+        for far in order:
+            base = lax.rem(group + far, groups) * GROUP
+            for near in range(GROUP):
+                if far or near:
+                    yield far, near, base + lax.rem(place + near, GROUP)
+
+    for _, _, peer in peers():
+        pl.semaphore_signal(barrier, inc=1, device_id=(peer,), device_id_type=MESH)
     loads = [
         pltpu.make_async_copy(source, target, local_sem.at[number])
         for number, (source, target) in enumerate(
             (
                 (shared_gate, sg),
                 (shared_up, su),
+                (shared_down, sd),
                 (expert_gate.at[0], eg),
                 (expert_up.at[0], eu),
-                (shared_down, sd),
                 (expert_down.at[0], ed),
             )
         )
@@ -535,12 +596,11 @@
     for load in loads:
         load.start()
 
-    rows = second[...]
+    smalls[0].wait()
     lines = lax.broadcasted_iota(jnp.int32, (routes.shape[1], PARTS * count), 0)
     lanes = lax.broadcasted_iota(jnp.int32, (routes.shape[1], PARTS * count), 1)
     pick = onehot(lines == me * count + lanes % count)
     routes_wide = dot(onehot_values(routes[...]), pick)
-    stacked = jnp.concatenate([rows[:, q * part : (q + 1) * part] for q in range(PARTS)], 0)
     line = lax.broadcasted_iota(jnp.int32, (total, tall), 0)
     lane = lax.broadcasted_iota(jnp.int32, (total, tall), 1)
     named = line < 0
@@ -551,60 +611,88 @@
     same = up_row // count == up_col // count
     before = dot(onehot(named), onehot(same & (up_row < up_col)))
     fits = (before == (line % MOST).astype(F32)) & (lane // count == (line % block) // MOST)
-    outgoing = dot(onehot(named & fits), stacked).astype(BF16)
-    sbuf[...] = outgoing.reshape(devices, block, part)
+    chosen = onehot(named & fits)
+    smalls[1].wait()
+    rows = second[...]
+    stacked = jnp.concatenate([rows[:, q * part : (q + 1) * part] for q in range(PARTS)], 0)
+    sbuf[...] = dot(chosen, stacked).astype(BF16).reshape(devices, block, part)
     pl.semaphore_wait(barrier, devices - 1)
 
-    def exchange(source_ref, target_ref, send, receive, offset, landing):
-        peer = (me + offset) % devices
+    def remote(source, target, send, receive, peer):
         return pltpu.make_async_remote_copy(
-            src_ref=source_ref.at[peer],
-            dst_ref=target_ref.at[landing],
-            send_sem=send.at[offset],
-            recv_sem=receive.at[offset],
+            src_ref=source,
+            dst_ref=target,
+            send_sem=send,
+            recv_sem=receive,
             device_id=(peer,),
             device_id_type=MESH,
         )
 
-    def start_all(source_ref, target_ref, send, receive):
-        def one(turn, carry):
-            offset = devices // 2 + (1 - 2 * (turn % 2)) * ((turn + 1) // 2)
-            exchange(source_ref, target_ref, send, receive, offset, me).start()
-            return carry
-
-        lax.fori_loop(0, devices - 1, one, 0)
-
-    def receive_all(source_ref, target_ref, send, receive):
-        def one(offset, carry):
-            origin = (me + devices - offset) % devices
-            exchange(source_ref, target_ref, send, receive, offset, origin).wait_recv()
-            return carry
-
-        lax.fori_loop(1, devices, one, 0)
-
-    def sent_all(source_ref, target_ref, send, receive):
-        def one(offset, carry):
-            exchange(source_ref, target_ref, send, receive, offset, me).wait_send()
-            return carry
-
-        lax.fori_loop(1, devices, one, 0)
-
-    there = (sbuf, rbuf, osend_sem, orecv_sem)
-    back = (pbuf, abuf, bsend_sem, brecv_sem)
+    before_me = lax.rem(group + groups - 1, groups) * GROUP + place
+    after_me = lax.rem(group + 1, groups) * GROUP + place
+    across_base = lax.rem(group + groups // 2, groups) * GROUP
+    next_base = lax.rem(group + 1 + groups // 2, groups) * GROUP
+
+    def hop(phase, source_ref):
+        return remote(
+            source_ref.at[pl.ds(across_base + GROUP - relayed, relayed)],
+            hops.at[phase],
+            send_sem.at[phase],
+            hop_recv_sem.at[phase],
+            before_me,
+        )
+
+    def start_all(phase, source_ref, target_ref):
+        sent = send_sem.at[phase], recv_sem.at[phase]
+        if relayed:
+            hop(phase, source_ref).start()
+        for far, near, peer in peers():
+            if relayed and far == groups // 2:
+                if near < GROUP - relayed:
+                    peer = across_base + near
+                    remote(source_ref.at[peer], target_ref.at[me], *sent, peer).start()
+            else:
+                remote(source_ref.at[peer], target_ref.at[me], *sent, peer).start()
+
+    def forward(phase, source_ref, target_ref):
+        if relayed:
+            hop(phase, source_ref).wait_recv()
+            for which in range(relayed):
+                remote(
+                    hops.at[phase, which],
+                    target_ref.at[after_me],
+                    hop_send_sem.at[phase],
+                    recv_sem.at[phase],
+                    next_base + GROUP - relayed + which,
+                ).start()
+
+    def everything(phase, source_ref, target_ref):
+        others = pl.ds(0, devices - 1)
+        return remote(
+            source_ref.at[others],
+            target_ref.at[others],
+            send_sem.at[phase],
+            recv_sem.at[phase],
+            before_me,
+        )
+
+    def sent_all(phase, source_ref, target_ref):
+        everything(phase, source_ref, target_ref).wait_send()
+        if relayed:
+            remote(
+                hops.at[phase],
+                target_ref.at[pl.ds(0, relayed)],
+                hop_send_sem.at[phase],
+                recv_sem.at[phase],
+                before_me,
+            ).wait_send()
+
+    there = (0, sbuf, rbuf)
+    back = (1, pbuf, abuf)
     start_all(*there)
     rbuf[me] = sbuf[me]
 
-    def gated(inputs, gate_ref, up_ref):
-        gate_part = dot(inputs, gate_ref[...])
-        up_part = dot(inputs, up_ref[...])
-        return (jax.nn.silu(gate_part) * up_part).astype(BF16)
-
-    loads[0].wait()
-    loads[1].wait()
-    shared_hidden = gated(rows, sg, su)
-    loads[4].wait()
-    shared = dot(shared_hidden, sd[...])
-
+    smalls[2].wait()
     across = lax.broadcasted_iota(jnp.int32, (tall, total), 1)
     down = lax.broadcasted_iota(jnp.int32, (tall, total), 0)
     named_t = across < 0
@@ -628,38 +716,48 @@
         down // count == (across % block) // MOST
     )
     weight_t = jnp.where(fits_t, weight_t, 0.0)
-    first, middle, last = thirds(weight_t)
+    weight_pieces = jnp.concatenate(thirds(weight_t), 0)
+
+    forward(*there)
+
+    def gated(inputs, gate_ref, up_ref):
+        gate_part = dot(inputs, gate_ref[...])
+        up_part = dot(inputs, up_ref[...])
+        return (jax.nn.silu(gate_part) * up_part).astype(BF16)
+
+    loads[0].wait()
+    loads[1].wait()
+    shared_hidden = gated(rows, sg, su)
+    loads[2].wait()
+    smalls[3].wait()
+    kept = residual[...].astype(F32) + dot(shared_hidden, sd[...])
 
     slots = devices * MOST
-    narrow = lax.broadcasted_iota(jnp.int32, (slots, total), 0)
-    broad = lax.broadcasted_iota(jnp.int32, (slots, total), 1)
-    tall_row = lax.broadcasted_iota(jnp.int32, (total, slots), 0)
-    tall_col = lax.broadcasted_iota(jnp.int32, (total, slots), 1)
-    takes = []
-    gives = []
+    row = lax.broadcasted_iota(jnp.int32, (total, total), 0)
+    col = lax.broadcasted_iota(jnp.int32, (total, total), 1)
+
+    def ordered(place):
+        return place % slots // MOST * block + place // slots * MOST + place % MOST
+
+    take = onehot(col == ordered(row))
+    give = onehot(row == ordered(col))
+
+    for load in loads[3:]:
+        load.wait()
+    everything(*there).wait_recv()
+    taken = dot(take, rbuf[...].reshape(total, part)).astype(BF16)
     for q in range(PARTS):
-        takes.append(onehot(broad == narrow // MOST * block + q * MOST + narrow % MOST))
-        gives.append(onehot(tall_row == tall_col // MOST * block + q * MOST + tall_col % MOST))
-
-    receive_all(*there)
-    received = rbuf[...].reshape(total, part)
-    for q in range(PARTS):
-        xfull[:, q * part : (q + 1) * part] = dot(takes[q], received).astype(BF16)
-    loads[2].wait()
-    loads[3].wait()
+        xfull[:, q * part : (q + 1) * part] = taken[q * slots : (q + 1) * slots]
     hidden = gated(xfull[...], eg, eu)
-    loads[5].wait()
-    produced = jnp.zeros((total, part), F32)
-    for q in range(PARTS):
-        result = dot(hidden, ed[:, q * part : (q + 1) * part]).astype(BF16)
-        produced = produced + dot(gives[q], result)
-    pbuf[...] = produced.astype(BF16).reshape(devices, block, part)
+    result = dot(hidden, ed[...]).astype(BF16)
+    result = jnp.concatenate([result[:, q * part : (q + 1) * part] for q in range(PARTS)], 0)
+    pbuf[...] = dot(give, result).astype(BF16).reshape(devices, block, part)
     start_all(*back)
     abuf[me] = pbuf[me]
-    receive_all(*back)
-    answers = abuf[...].reshape(total, part)
-    routed = dot(first, answers) + dot(middle, answers) + dot(last, answers)
-    kept = residual[...].astype(F32) + shared
+    forward(*back)
+    everything(*back).wait_recv()
+    pieces = dot(weight_pieces, abuf[...].reshape(total, part))
+    routed = pieces[:tall] + pieces[tall : 2 * tall] + pieces[2 * tall :]
     for q in range(PARTS):
         cut = slice(q * part, (q + 1) * part)
         out[:, cut] = (kept[:, cut] + routed[q * count : (q + 1) * count]).astype(BF16)
@@ -673,26 +771,30 @@
     hbm = pl.BlockSpec(memory_space=pl.ANY)
     dma = pltpu.SemaphoreType.DMA
     exchange = pltpu.VMEM((devices, PARTS * MOST, width // PARTS), BF16)
+    smalls = (second, residual, routes, weights)
     return pl.pallas_call(
         functools.partial(experts_kernel, devices),
         out_shape=jax.ShapeDtypeStruct((count, width), BF16),
-        in_specs=[vmem] * 4 + [hbm] * 6,
+        in_specs=[hbm] * 10,
         out_specs=vmem,
-        scratch_shapes=[pltpu.VMEM(m.shape[-2:], BF16) for m in matrices]
+        scratch_shapes=[pltpu.VMEM(array.shape, array.dtype) for array in smalls]
+        + [pltpu.VMEM(m.shape[-2:], BF16) for m in matrices]
         + [exchange] * 4
         + [
+            pltpu.VMEM((2, GROUP // 2, PARTS * MOST, width // PARTS), BF16),
             pltpu.VMEM((devices * MOST, width), BF16),
+            dma((4,)),
             dma((6,)),
-            dma((devices,)),
-            dma((devices,)),
-            dma((devices,)),
-            dma((devices,)),
+            dma((2,)),
+            dma((2,)),
+            dma((2,)),
+            dma((2,)),
         ],
         compiler_params=pltpu.CompilerParams(
             collective_id=1, has_side_effects=True, vmem_limit_bytes=VMEM_BYTES
         ),
         name="experts",
-    )(second, residual, routes, weights, *matrices)
+    )(*smalls, *matrices)
 
 
 def per_device(
@@ -724,11 +826,9 @@
     devices = lax.axis_size("ep")
     vectors = project(
         devices,
+        (w_receptance, w_key, w_value),
         tokens,
         first_gain[None, :],
-        w_receptance,
-        w_key,
-        w_value,
         decay_down.T,
         decay_up,
         decay_base[None, :],

time: 75.6 us -> 68.1 us (0.901)
  Pallas kernels: 73.1 us -> 65.6 us
    pallas_call x1, Pallas kernels: 35.8 us -> 30.3 us  [experts(): pl.pallas_call(functools.partial(experts_kernel, devices), out_shape=jax....]
    pallas_call x1, Pallas kernels: 28.9 us -> 26.9 us  [project(): pl.pallas_call(functools.partial(project_kernel, devices), out_shape=jax....]
where the time goes in v2:
time: 68.1 us; the launch traced here: 67.7 us
  Pallas kernels  65.6 us (96%)
  local copies, waits for them, and re-layouts  1.47 us (2%)
    pallas_call x1, Pallas kernels, experts(): pl.pallas_call(functools.partial(experts_kernel, devices), out_shape=jax....  30.3 us
    pallas_call x1, Pallas kernels, project(): pl.pallas_call(functools.partial(project_kernel, devices), out_shape=jax....  26.9 us
    pallas_call x1, Pallas kernels, mixer(): pl.pallas_call(mixer_kernel, out_shape=[jax.ShapeDtypeStruct(state.shape,...  8.4 us
    unnamed x1, local copies, waits for them, and re-layouts  1.47 us

profile of v2, /device:TPU:0, one launch (start us, length us, event | category | flops | bytes accessed | tf_op | source)
XLA Modules:
  0.0 67.7 jit_solution(3349797640356758138)
XLA Ops:
  0.6 26.9 %project.1.vectors_in = f32[6,16,16,64]{3,2,1,0:T(8,128)} custom-call(bf16[16,2048]{1,0:T(8,128)(2,1)} %tokens.1, f32[1,2048]{1,0:T(1,128)} %bitcast.12, bf16[64,2048]{1,0:T(8,128)(2,1)} %bitcast.10, bf16[64,1024]{1,0:T(8,128)(2,1)} %decay_up_in.1, f32[1,1024]{1,0:T(1,128)} %bitcast.17, bf16[64,2048]{1,0:T(8,128)(2,1)} %bitcast.11, ...), custom_call_target="tpu_custom_call" | custom-call | tf_op jit(solution)/shard_map/project/pallas_call | solution.py:291
  27.6 8.4 %mixer.1 = (f32[16,16,4096]{2,1,0:T(8,128)}, bf16[16,2048]{1,0:T(8,128)(2,1)}, bf16[16,2048]{1,0:T(8,128)(2,1)}) custom-call(f32[6,16,16,64]{3,2,1,0:T(8,128)} %project.1.vectors_in, f32[16,16,4096]{2,1,0:T(8,128)} %state_in.1, f32[1,1024]{1,0:T(1,128)} %bitcast.16, bf16[16,2048]{1,0:T(8,128)(2,1)} %tokens.1, bf16[1024,2048]{1,0:T(8,128)(2,1)} %w_output.1, ...), custom_call_target="tpu_custom_call" | custom-call | tf_op jit(solution)/shard_map/mixer/pallas_call | solution.py:470
  36.0 30.3 %experts.1 = bf16[16,2048]{1,0:T(8,128)(2,1)} custom-call(bf16[16,2048]{1,0:T(8,128)(2,1)} %get-tuple-element.5.second_in, bf16[16,2048]{1,0:T(8,128)(2,1)} %get-tuple-element.6.residual_in, s32[4,512]{1,0:T(4,128)} %bitcast.14, f32[4,512]{1,0:T(4,128)} %bitcast.15, bf16[2048,512]{1,0:T(8,128)(2,1)} %shared_gate.1, bf16[2048,512]{1,0:T(8,128)(2,1)} %shared_up.1, ...), custom_call_target="tpu_custom_call" | custom-call | tf_op jit(solution)/shard_map/experts/pallas_call | solution.py:775
  66.3 1.5 %copy.27 = bf16[16,2048]{1,0:T(8,128)(2,1)} copy(bf16[16,2048]{1,0:T(8,128)(2,1)} %experts.1) | data formatting | bytes 131072

commit v3 on v2

--- a/solution.py
+++ b/solution.py
@@ -11,7 +11,6 @@
 TOPK = 4
 MOST = 4
 GROUP = 8
-PARTS = 4
 SPAN = 256
 SPLIT = 2
 NORM_EPS = 1e-06
@@ -19,7 +18,7 @@
 MESH = pl.DeviceIdType.MESH
 F32 = jnp.float32
 BF16 = jnp.bfloat16
-VMEM_BYTES = 60 * 1024 * 1024
+VMEM_BYTES = 40 * 1024 * 1024
 
 
 def dot(a, b):
@@ -47,8 +46,20 @@
     w_r,
     w_k,
     w_v,
+    state_in,
+    w_output_in,
+    head_gain_in,
+    second_gain_in,
+    routes_in,
+    route_weights_in,
     out,
     tokens,
+    state,
+    w_output,
+    head_gain,
+    second_gain,
+    routes,
+    route_weights,
     gain,
     decay_down,
     decay_up,
@@ -63,6 +74,7 @@
     xbuf,
     psend,
     precv,
+    ahead_sem,
     small_sem,
     local_sem,
     wsend_sem,
@@ -132,6 +144,21 @@
                 ).start()
     for small in smalls[2:]:
         small.start()
+    ahead = [
+        pltpu.make_async_copy(source, target, ahead_sem.at[number])
+        for number, (source, target) in enumerate(
+            (
+                (state_in, state),
+                (w_output_in, w_output),
+                (head_gain_in, head_gain),
+                (second_gain_in, second_gain),
+                (routes_in, routes),
+                (route_weights_in, route_weights),
+            )
+        )
+    ]
+    for load in ahead:
+        load.start()
 
     def loaded(number):
         span = stage.at[pl.ds(number * SPLIT, SPLIT)]
@@ -276,9 +303,11 @@
     remote(xbuf.at[others], xbuf.at[others], xsend_sem, xrecv_sem, partner).wait_send()
     span = psend.at[:, others]
     remote(span, span, psend_sem, precv_sem.at[0], partner).wait_send()
-
-
-def project(devices, weights, *smalls):
+    for load in ahead:
+        load.wait()
+
+
+def project(devices, weights, aheads, *smalls):
     count, width = smalls[0].shape
     rows, mix = weights[0].shape
     groups = devices // GROUP
@@ -286,14 +315,15 @@
     piece = mix // 2 // SPLIT
     pieces = 3 * SPLIT
     vmem = pl.BlockSpec(memory_space=pltpu.VMEM)
-    hbm = pl.BlockSpec(memory_space=pl.ANY)
+    hbm = pl.BlockSpec(memory_space=pltpu.HBM)
     dma = pltpu.SemaphoreType.DMA
     return pl.pallas_call(
         functools.partial(project_kernel, devices),
-        out_shape=jax.ShapeDtypeStruct((6, count, mix // HEAD, HEAD), F32),
-        in_specs=[hbm] * 12,
-        out_specs=vmem,
-        scratch_shapes=[pltpu.VMEM(array.shape, array.dtype) for array in smalls]
+        out_shape=[pltpu.VMEM((6, count, mix // HEAD, HEAD), F32)]
+        + [pltpu.VMEM(array.shape, array.dtype) for array in (smalls[0],) + aheads],
+        in_specs=[hbm] * (12 + len(aheads)),
+        out_specs=[vmem] * (2 + len(aheads)),
+        scratch_shapes=[pltpu.VMEM(array.shape, array.dtype) for array in smalls[1:]]
         + [
             pltpu.VMEM((pieces, 2, rows, piece), BF16),
             pltpu.VMEM((pieces, GROUP * rows, piece), BF16),
@@ -301,6 +331,7 @@
             pltpu.VMEM((members, count, width // groups), BF16),
             pltpu.VMEM((pieces, members, count, piece), BF16),
             pltpu.VMEM((pieces, members, count, piece), BF16),
+            dma((len(aheads),)),
             dma((9,)),
             dma((3,)),
             dma,
@@ -314,7 +345,7 @@
             collective_id=0, has_side_effects=True, vmem_limit_bytes=VMEM_BYTES
         ),
         name="project",
-    )(*smalls, *weights)
+    )(*map(pinned, (*smalls, *weights, *aheads)))
 
 
 def split_sum(values, ones):
@@ -324,8 +355,9 @@
 
 
 def mixer_kernel(
-    vectors_in,
-    state_in,
+    steps,
+    vectors,
+    state,
     head_gain,
     tokens,
     w_output,
@@ -333,21 +365,14 @@
     new_state,
     residual,
     second,
-    vectors,
-    state,
     fresh_out,
-    wbuf,
     mixed,
     work,
     sums,
-    vec_sem,
-    in_sem,
     out_sem,
-    w_sem,
 ):
     _, count, heads, _ = vectors.shape
     entries = state.shape[2]
-    steps = in_sem.shape[0]
     per_step = count // steps
     span = SPAN
     tiles = entries // span
@@ -356,18 +381,6 @@
     def rows_of(step):
         return pl.ds(step * per_step, per_step)
 
-    def state_load(step):
-        return pltpu.make_async_copy(
-            state_in.at[rows_of(step)], state.at[rows_of(step)], in_sem.at[step]
-        )
-
-    vector_load = pltpu.make_async_copy(vectors_in, vectors, vec_sem)
-    weight_load = pltpu.make_async_copy(w_output, wbuf, w_sem)
-    vector_load.start()
-    for step in range(steps):
-        state_load(step).start()
-    weight_load.start()
-
     row = lax.broadcasted_iota(jnp.int32, (span, span), 0)
     col = lax.broadcasted_iota(jnp.int32, (span, span), 1)
     ones = (row // HEAD == col // HEAD).astype(F32).astype(BF16)
@@ -376,10 +389,7 @@
     def widen(inputs):
         return jnp.concatenate([inputs] * copies, axis=1)
 
-    vector_load.wait()
-
     def one_step(step, carry):
-        state_load(step).wait()
         size = tiles * heads
         kept = []
         for place in range(per_step):
@@ -451,8 +461,7 @@
     owner = lax.broadcasted_iota(jnp.int32, (count, count * heads), 1) // heads
     token = lax.broadcasted_iota(jnp.int32, (count, count * heads), 0)
     rows = dot((owner == token).astype(F32).astype(BF16), kept).astype(BF16)
-    weight_load.wait()
-    after = (tokens[...].astype(F32) + dot(rows, wbuf[...])).astype(BF16)
+    after = (tokens[...].astype(F32) + dot(rows, w_output[...])).astype(BF16)
     residual[...] = after
     second[...] = rms_scale(after, second_gain[...]).astype(BF16)
     pltpu.make_async_copy(fresh_out, new_state, out_sem).wait()
@@ -468,25 +477,19 @@
     hbm = pl.BlockSpec(memory_space=pl.ANY)
     dma = pltpu.SemaphoreType.DMA
     return pl.pallas_call(
-        mixer_kernel,
+        functools.partial(mixer_kernel, steps),
         out_shape=[
             jax.ShapeDtypeStruct(state.shape, F32),
-            jax.ShapeDtypeStruct((count, width), BF16),
-            jax.ShapeDtypeStruct((count, width), BF16),
+            pltpu.VMEM((count, width), BF16),
+            pltpu.VMEM((count, width), BF16),
         ],
-        in_specs=[hbm, hbm, vmem, vmem, hbm, vmem],
+        in_specs=[vmem] * 6,
         out_specs=[hbm, vmem, vmem],
         scratch_shapes=[
-            pltpu.VMEM(vectors.shape, F32),
             pltpu.VMEM(state.shape, F32),
-            pltpu.VMEM(state.shape, F32),
-            pltpu.VMEM(w_output.shape, BF16),
             pltpu.VMEM((count, heads, HEAD), F32),
             pltpu.VMEM((rows, SPAN), BF16),
             pltpu.VMEM((rows, SPAN), F32),
-            dma,
-            dma((steps,)),
-            dma,
             dma,
         ],
         compiler_params=pltpu.CompilerParams(vmem_limit_bytes=VMEM_BYTES),
@@ -511,10 +514,10 @@
 
 def experts_kernel(
     devices,
-    second_in,
-    residual_in,
-    routes_in,
-    route_weights_in,
+    second,
+    residual,
+    routes,
+    route_weights,
     shared_gate,
     shared_up,
     shared_down,
@@ -522,10 +525,6 @@
     expert_up,
     expert_down,
     out,
-    second,
-    residual,
-    routes,
-    route_weights,
     sg,
     su,
     sd,
@@ -536,49 +535,26 @@
     rbuf,
     pbuf,
     abuf,
-    hops,
-    xfull,
-    small_sem,
     local_sem,
     send_sem,
     recv_sem,
-    hop_send_sem,
-    hop_recv_sem,
 ):
     count, width = second.shape
-    part = width // PARTS
-    block = PARTS * MOST
-    total = devices * block
-    tall = PARTS * count
+    total = devices * MOST
     groups = devices // GROUP
-    relayed = 0
     me = lax.axis_index("ep")
     group = me // GROUP
     place = me % GROUP
     barrier = pltpu.get_barrier_semaphore()
-    smalls = [
-        pltpu.make_async_copy(source, target, small_sem.at[number])
-        for number, (source, target) in enumerate(
-            (
-                (routes_in, routes),
-                (second_in, second),
-                (route_weights_in, route_weights),
-                (residual_in, residual),
-            )
-        )
-    ]
-    for small in smalls:
-        small.start()
-
     def peers():
         order = sorted(range(groups), key=lambda g: (-min(g, groups - g), g))
         for far in order:
             base = lax.rem(group + far, groups) * GROUP
             for near in range(GROUP):
                 if far or near:
-                    yield far, near, base + lax.rem(place + near, GROUP)
-
-    for _, _, peer in peers():
+                    yield base + lax.rem(place + near, GROUP)
+
+    for peer in peers():
         pl.semaphore_signal(barrier, inc=1, device_id=(peer,), device_id_type=MESH)
     loads = [
         pltpu.make_async_copy(source, target, local_sem.at[number])
@@ -596,26 +572,20 @@
     for load in loads:
         load.start()
 
-    smalls[0].wait()
-    lines = lax.broadcasted_iota(jnp.int32, (routes.shape[1], PARTS * count), 0)
-    lanes = lax.broadcasted_iota(jnp.int32, (routes.shape[1], PARTS * count), 1)
-    pick = onehot(lines == me * count + lanes % count)
+    lines = lax.broadcasted_iota(jnp.int32, (routes.shape[1], count), 0)
+    lanes = lax.broadcasted_iota(jnp.int32, (routes.shape[1], count), 1)
+    pick = onehot(lines == me * count + lanes)
     routes_wide = dot(onehot_values(routes[...]), pick)
-    line = lax.broadcasted_iota(jnp.int32, (total, tall), 0)
-    lane = lax.broadcasted_iota(jnp.int32, (total, tall), 1)
+    line = lax.broadcasted_iota(jnp.int32, (total, count), 0)
     named = line < 0
     for j in range(TOPK):
-        named = named | (routes_wide[j : j + 1, :] == (line // block).astype(F32))
-    up_row = lax.broadcasted_iota(jnp.int32, (tall, tall), 0)
-    up_col = lax.broadcasted_iota(jnp.int32, (tall, tall), 1)
-    same = up_row // count == up_col // count
-    before = dot(onehot(named), onehot(same & (up_row < up_col)))
-    fits = (before == (line % MOST).astype(F32)) & (lane // count == (line % block) // MOST)
-    chosen = onehot(named & fits)
-    smalls[1].wait()
+        named = named | (routes_wide[j : j + 1, :] == (line // MOST).astype(F32))
+    up_row = lax.broadcasted_iota(jnp.int32, (count, count), 0)
+    up_col = lax.broadcasted_iota(jnp.int32, (count, count), 1)
+    before = dot(onehot(named), onehot(up_row < up_col))
+    chosen = onehot(named & (before == (line % MOST).astype(F32)))
     rows = second[...]
-    stacked = jnp.concatenate([rows[:, q * part : (q + 1) * part] for q in range(PARTS)], 0)
-    sbuf[...] = dot(chosen, stacked).astype(BF16).reshape(devices, block, part)
+    sbuf[...] = dot(chosen, rows).astype(BF16).reshape(devices, MOST, width)
     pl.semaphore_wait(barrier, devices - 1)
 
     def remote(source, target, send, receive, peer):
@@ -628,43 +598,15 @@
             device_id_type=MESH,
         )
 
-    before_me = lax.rem(group + groups - 1, groups) * GROUP + place
-    after_me = lax.rem(group + 1, groups) * GROUP + place
-    across_base = lax.rem(group + groups // 2, groups) * GROUP
-    next_base = lax.rem(group + 1 + groups // 2, groups) * GROUP
-
-    def hop(phase, source_ref):
-        return remote(
-            source_ref.at[pl.ds(across_base + GROUP - relayed, relayed)],
-            hops.at[phase],
-            send_sem.at[phase],
-            hop_recv_sem.at[phase],
-            before_me,
-        )
-
     def start_all(phase, source_ref, target_ref):
-        sent = send_sem.at[phase], recv_sem.at[phase]
-        if relayed:
-            hop(phase, source_ref).start()
-        for far, near, peer in peers():
-            if relayed and far == groups // 2:
-                if near < GROUP - relayed:
-                    peer = across_base + near
-                    remote(source_ref.at[peer], target_ref.at[me], *sent, peer).start()
-            else:
-                remote(source_ref.at[peer], target_ref.at[me], *sent, peer).start()
-
-    def forward(phase, source_ref, target_ref):
-        if relayed:
-            hop(phase, source_ref).wait_recv()
-            for which in range(relayed):
-                remote(
-                    hops.at[phase, which],
-                    target_ref.at[after_me],
-                    hop_send_sem.at[phase],
-                    recv_sem.at[phase],
-                    next_base + GROUP - relayed + which,
-                ).start()
+        for peer in peers():
+            remote(
+                source_ref.at[peer],
+                target_ref.at[me],
+                send_sem.at[phase],
+                recv_sem.at[phase],
+                peer,
+            ).start()
 
     def everything(phase, source_ref, target_ref):
         others = pl.ds(0, devices - 1)
@@ -673,52 +615,34 @@
             target_ref.at[others],
             send_sem.at[phase],
             recv_sem.at[phase],
-            before_me,
+            lax.rem(me + 1, devices),
         )
-
-    def sent_all(phase, source_ref, target_ref):
-        everything(phase, source_ref, target_ref).wait_send()
-        if relayed:
-            remote(
-                hops.at[phase],
-                target_ref.at[pl.ds(0, relayed)],
-                hop_send_sem.at[phase],
-                recv_sem.at[phase],
-                before_me,
-            ).wait_send()
 
     there = (0, sbuf, rbuf)
     back = (1, pbuf, abuf)
     start_all(*there)
     rbuf[me] = sbuf[me]
 
-    smalls[2].wait()
-    across = lax.broadcasted_iota(jnp.int32, (tall, total), 1)
-    down = lax.broadcasted_iota(jnp.int32, (tall, total), 0)
+    across = lax.broadcasted_iota(jnp.int32, (count, total), 1)
     named_t = across < 0
     turned = (((1,), (1,)), ((), ()))
-    lines_t = lax.broadcasted_iota(jnp.int32, (tall, routes.shape[1]), 1)
-    lanes_t = lax.broadcasted_iota(jnp.int32, (tall, routes.shape[1]), 0)
-    pick_t = onehot(lines_t == me * count + lanes_t % count)
+    lines_t = lax.broadcasted_iota(jnp.int32, (count, routes.shape[1]), 1)
+    lanes_t = lax.broadcasted_iota(jnp.int32, (count, routes.shape[1]), 0)
+    pick_t = onehot(lines_t == me * count + lanes_t)
 
     def picked(values):
         return lax.dot_general(pick_t, values, turned, preferred_element_type=F32)
 
     routes_tall = picked(onehot_values(routes[...]))
     weights_tall = sum(picked(piece) for piece in thirds(route_weights[...]))
-    weight_t = jnp.zeros((tall, total), F32)
+    weight_t = jnp.zeros((count, total), F32)
     for j in range(TOPK):
-        hit = routes_tall[:, j : j + 1] == (across // block).astype(F32)
+        hit = routes_tall[:, j : j + 1] == (across // MOST).astype(F32)
         named_t = named_t | hit
         weight_t = weight_t + jnp.where(hit, weights_tall[:, j : j + 1], 0.0)
-    before_t = dot(onehot(same & (up_col < up_row)), onehot(named_t))
-    fits_t = (before_t == (across % MOST).astype(F32)) & (
-        down // count == (across % block) // MOST
-    )
-    weight_t = jnp.where(fits_t, weight_t, 0.0)
+    before_t = dot(onehot(up_col < up_row), onehot(named_t))
+    weight_t = jnp.where(before_t == (across % MOST).astype(F32), weight_t, 0.0)
     weight_pieces = jnp.concatenate(thirds(weight_t), 0)
-
-    forward(*there)
 
     def gated(inputs, gate_ref, up_ref):
         gate_part = dot(inputs, gate_ref[...])
@@ -729,64 +653,38 @@
     loads[1].wait()
     shared_hidden = gated(rows, sg, su)
     loads[2].wait()
-    smalls[3].wait()
     kept = residual[...].astype(F32) + dot(shared_hidden, sd[...])
-
-    slots = devices * MOST
-    row = lax.broadcasted_iota(jnp.int32, (total, total), 0)
-    col = lax.broadcasted_iota(jnp.int32, (total, total), 1)
-
-    def ordered(place):
-        return place % slots // MOST * block + place // slots * MOST + place % MOST
-
-    take = onehot(col == ordered(row))
-    give = onehot(row == ordered(col))
 
     for load in loads[3:]:
         load.wait()
     everything(*there).wait_recv()
-    taken = dot(take, rbuf[...].reshape(total, part)).astype(BF16)
-    for q in range(PARTS):
-        xfull[:, q * part : (q + 1) * part] = taken[q * slots : (q + 1) * slots]
-    hidden = gated(xfull[...], eg, eu)
-    result = dot(hidden, ed[...]).astype(BF16)
-    result = jnp.concatenate([result[:, q * part : (q + 1) * part] for q in range(PARTS)], 0)
-    pbuf[...] = dot(give, result).astype(BF16).reshape(devices, block, part)
+    hidden = gated(rbuf[...].reshape(total, width), eg, eu)
+    pbuf[...] = dot(hidden, ed[...]).astype(BF16).reshape(devices, MOST, width)
     start_all(*back)
     abuf[me] = pbuf[me]
-    forward(*back)
     everything(*back).wait_recv()
-    pieces = dot(weight_pieces, abuf[...].reshape(total, part))
-    routed = pieces[:tall] + pieces[tall : 2 * tall] + pieces[2 * tall :]
-    for q in range(PARTS):
-        cut = slice(q * part, (q + 1) * part)
-        out[:, cut] = (kept[:, cut] + routed[q * count : (q + 1) * count]).astype(BF16)
-    sent_all(*there)
-    sent_all(*back)
+    pieces = dot(weight_pieces, abuf[...].reshape(total, width))
+    routed = pieces[:count] + pieces[count : 2 * count] + pieces[2 * count :]
+    out[...] = (kept + routed).astype(BF16)
+    everything(*there).wait_send()
+    everything(*back).wait_send()
 
 
 def experts(devices, second, residual, routes, weights, *matrices):
     count, width = second.shape
     vmem = pl.BlockSpec(memory_space=pltpu.VMEM)
-    hbm = pl.BlockSpec(memory_space=pl.ANY)
+    hbm = pl.BlockSpec(memory_space=pltpu.HBM)
     dma = pltpu.SemaphoreType.DMA
-    exchange = pltpu.VMEM((devices, PARTS * MOST, width // PARTS), BF16)
-    smalls = (second, residual, routes, weights)
+    exchange = pltpu.VMEM((devices, MOST, width), BF16)
     return pl.pallas_call(
         functools.partial(experts_kernel, devices),
-        out_shape=jax.ShapeDtypeStruct((count, width), BF16),
-        in_specs=[hbm] * 10,
+        out_shape=pltpu.VMEM((count, width), BF16),
+        in_specs=[vmem] * 4 + [hbm] * 6,
         out_specs=vmem,
-        scratch_shapes=[pltpu.VMEM(array.shape, array.dtype) for array in smalls]
-        + [pltpu.VMEM(m.shape[-2:], BF16) for m in matrices]
+        scratch_shapes=[pltpu.VMEM(m.shape[-2:], BF16) for m in matrices]
         + [exchange] * 4
         + [
-            pltpu.VMEM((2, GROUP // 2, PARTS * MOST, width // PARTS), BF16),
-            pltpu.VMEM((devices * MOST, width), BF16),
-            dma((4,)),
             dma((6,)),
-            dma((2,)),
-            dma((2,)),
             dma((2,)),
             dma((2,)),
         ],
@@ -794,7 +692,11 @@
             collective_id=1, has_side_effects=True, vmem_limit_bytes=VMEM_BYTES
         ),
         name="experts",
-    )(*smalls, *matrices)
+    )(second, residual, routes, weights, *map(pinned, matrices))
+
+
+def pinned(array):
+    return pltpu.with_memory_space_constraint(array, pltpu.HBM)
 
 
 def per_device(
@@ -824,9 +726,17 @@
     route_weights,
 ):
     devices = lax.axis_size("ep")
-    vectors = project(
+    vectors, *ahead = project(
         devices,
         (w_receptance, w_key, w_value),
+        (
+            recurrent_state,
+            w_output,
+            head_gain[None, :],
+            second_gain[None, :],
+            routes.T,
+            route_weights.T,
+        ),
         tokens,
         first_gain[None, :],
         decay_down.T,
@@ -837,20 +747,14 @@
         rate_base[None, :],
         key_scale[None, :],
     )
-    new_state, residual, second = mixer(
-        vectors,
-        recurrent_state,
-        head_gain[None, :],
-        tokens,
-        w_output,
-        second_gain[None, :],
-    )
+    tokens, state, w_output, head_gain, second_gain, routes, route_weights = ahead
+    new_state, residual, second = mixer(vectors, state, head_gain, tokens, w_output, second_gain)
     new_tokens = experts(
         devices,
         second,
         residual,
-        routes.T,
-        route_weights.T,
+        routes,
+        route_weights,
         shared_gate,
         shared_up,
         shared_down,

time: 68.1 us -> 61.7 us (0.906)
  Pallas kernels: 65.6 us -> 60.1 us
  local copies, waits for them, and re-layouts: 1.47 us -> 0.63 us
    pallas_call x3, Pallas kernels: 65.6 us -> 60.1 us  [the longest x1 29 us: experts(): pl.pallas_call(functools.partial(experts_kernel, devices), out_shape=pltp...]
    unnamed x1, local copies, waits for them, and re-layouts: 1.47 us -> 0.63 us
where the time goes in v3:
time: 61.7 us; the launch traced here: 61.4 us
  Pallas kernels  60.1 us (97%)
  between operations  0.66 us (1%)
  local copies, waits for them, and re-layouts  0.63 us (1%)
    pallas_call x1, Pallas kernels, experts(): pl.pallas_call(functools.partial(experts_kernel, devices), out_shape=pltp...  29 us
    pallas_call x1, Pallas kernels, project(): pl.pallas_call(functools.partial(project_kernel, devices), out_shape=[plt...  26.1 us
    pallas_call x1, Pallas kernels, mixer(): pl.pallas_call(functools.partial(mixer_kernel, steps), out_shape=[jax.Sha...  5.03 us

profile of v3, /device:TPU:0, one launch (start us, length us, event | category | flops | bytes accessed | tf_op | source)
XLA Modules:
  0.0 61.4 jit_solution(14793867827294227023)
XLA Ops:
  0.6 26.1 %project.1 = (f32[6,16,16,64]{3,2,1,0:T(8,128)S(1)}, bf16[16,2048]{1,0:T(8,128)(2,1)S(1)}, f32[16,16,4096]{2,1,0:T(8,128)S(1)}, bf16[1024,2048]{1,0:T(8,128)(2,1...) custom-call(bf16[16,2048]{1,0:T(8,128)(2,1)} %tokens_in.1, ...), custom_call_target="tpu_custom_call" | custom-call | tf_op jit(solution)/shard_map/project/pallas_call | solution.py:320
  26.8 5.0 %mixer.1 = (f32[16,16,4096]{2,1,0:T(8,128)}, bf16[16,2048]{1,0:T(8,128)(2,1)S(1)}, bf16[16,2048]{1,0:T(8,128)(2,1)S(1)}) custom-call(f32[6,16,16,64]{3,2,1,0:T(8,128)S(1)} %get-tuple-element.13.vectors, f32[16,16,4096]{2,1,0:T(8,128)S(1)} %get-tuple-element.14.state, f32[1,1024]{1,0:T(1,128)S(1)} %get-tuple-element.15.head_gain, ...), custom_call_target="tpu_custom_call" | custom-call | tf_op jit(solution)/shard_map/mixer/pallas_call | solution.py:479
  31.8 29.0 %experts.1 = bf16[16,2048]{1,0:T(8,128)(2,1)S(1)} custom-call(bf16[16,2048]{1,0:T(8,128)(2,1)S(1)} %get-tuple-element.19.second, bf16[16,2048]{1,0:T(8,128)(2,1)S(1)} %get-tuple-element.20.residual, s32[4,512]{1,0:T(4,128)S(1)} %get-tuple-element.21.routes, f32[4,512]{1,0:T(4,128)S(1)} %get-tuple-element.22.route_weights, bf16[2048,512]{1,0:T(8,128)(2,1)} %shared_gate.1, ...), custom_call_target="tpu_custom_call" | custom-call | tf_op jit(solution)/shard_map/experts/pallas_call | solution.py:679
  60.8 0.6 %copy.27 = bf16[16,2048]{1,0:T(8,128)(2,1)} copy(bf16[16,2048]{1,0:T(8,128)(2,1)S(1)} %experts.1) | data formatting | bytes 131072

commit v4 on v3

--- a/solution.py
+++ b/solution.py
@@ -18,7 +18,8 @@
 MESH = pl.DeviceIdType.MESH
 F32 = jnp.float32
 BF16 = jnp.bfloat16
-VMEM_BYTES = 40 * 1024 * 1024
+VMEM_BYTES = 57 * 1024 * 1024
+CLOSE_BYTES = 16 * 1024 * 1024
 
 
 def dot(a, b):
@@ -83,6 +84,7 @@
     xrecv_sem,
     psend_sem,
     precv_sem,
+    between,
 ):
     rows, mix = w_r.shape
     half = mix // 2
@@ -250,6 +252,9 @@
     put(4, jax.nn.sigmoid(rate_base[...] + dot(rate_low, rate_up[...])), 0)
     relay(2)
     direct(5)
+    for load in ahead[4:]:
+        load.wait()
+    between()
 
     others = pl.ds(0, members - 1)
     remote(xbuf.at[others], xbuf.at[others], xsend_sem, xrecv_sem, partner).wait_recv()
@@ -303,49 +308,8 @@
     remote(xbuf.at[others], xbuf.at[others], xsend_sem, xrecv_sem, partner).wait_send()
     span = psend.at[:, others]
     remote(span, span, psend_sem, precv_sem.at[0], partner).wait_send()
-    for load in ahead:
+    for load in ahead[:4]:
         load.wait()
-
-
-def project(devices, weights, aheads, *smalls):
-    count, width = smalls[0].shape
-    rows, mix = weights[0].shape
-    groups = devices // GROUP
-    members = 2 * groups
-    piece = mix // 2 // SPLIT
-    pieces = 3 * SPLIT
-    vmem = pl.BlockSpec(memory_space=pltpu.VMEM)
-    hbm = pl.BlockSpec(memory_space=pltpu.HBM)
-    dma = pltpu.SemaphoreType.DMA
-    return pl.pallas_call(
-        functools.partial(project_kernel, devices),
-        out_shape=[pltpu.VMEM((6, count, mix // HEAD, HEAD), F32)]
-        + [pltpu.VMEM(array.shape, array.dtype) for array in (smalls[0],) + aheads],
-        in_specs=[hbm] * (12 + len(aheads)),
-        out_specs=[vmem] * (2 + len(aheads)),
-        scratch_shapes=[pltpu.VMEM(array.shape, array.dtype) for array in smalls[1:]]
-        + [
-            pltpu.VMEM((pieces, 2, rows, piece), BF16),
-            pltpu.VMEM((pieces, GROUP * rows, piece), BF16),
-            pltpu.VMEM((groups, count, width // groups), BF16),
-            pltpu.VMEM((members, count, width // groups), BF16),
-            pltpu.VMEM((pieces, members, count, piece), BF16),
-            pltpu.VMEM((pieces, members, count, piece), BF16),
-            dma((len(aheads),)),
-            dma((9,)),
-            dma((3,)),
-            dma,
-            dma((3 * pieces,)),
-            dma,
-            dma,
-            dma,
-            dma((pieces,)),
-        ],
-        compiler_params=pltpu.CompilerParams(
-            collective_id=0, has_side_effects=True, vmem_limit_bytes=VMEM_BYTES
-        ),
-        name="project",
-    )(*map(pinned, (*smalls, *weights, *aheads)))
 
 
 def split_sum(values, ones):
@@ -354,88 +318,67 @@
     return dot(high, ones) + dot(low, ones)
 
 
-def mixer_kernel(
-    steps,
-    vectors,
-    state,
-    head_gain,
-    tokens,
-    w_output,
-    second_gain,
-    new_state,
-    residual,
-    second,
-    fresh_out,
-    mixed,
-    work,
-    sums,
-    out_sem,
-):
+def mixer_setup(vectors, state):
     _, count, heads, _ = vectors.shape
-    entries = state.shape[2]
-    per_step = count // steps
-    span = SPAN
-    tiles = entries // span
-    copies = span // HEAD
-
-    def rows_of(step):
-        return pl.ds(step * per_step, per_step)
-
-    row = lax.broadcasted_iota(jnp.int32, (span, span), 0)
-    col = lax.broadcasted_iota(jnp.int32, (span, span), 1)
-    ones = (row // HEAD == col // HEAD).astype(F32).astype(BF16)
-    lane = lax.broadcasted_iota(jnp.int32, (heads, span), 1)
+    tiles = state.shape[2] // SPAN
+    copies = SPAN // HEAD
+    lane = lax.broadcasted_iota(jnp.int32, (heads, SPAN), 1)
 
     def widen(inputs):
         return jnp.concatenate([inputs] * copies, axis=1)
 
+    def pick(i):
+        return lane % HEAD == i * copies + lane // HEAD
+
+    def directed(number):
+        scaled = vectors[5, number]
+        return scaled / jnp.sqrt(jnp.sum(scaled * scaled, axis=-1, keepdims=True) + 1.0)
+
+    return count, heads, tiles, copies, widen, pick, directed
+
+
+def mixer_read(vectors, state, head_gain, tokens, w_output, second_gain, mixed, work, sums):
+    count, heads, tiles, copies, widen, pick, directed = mixer_setup(vectors, state)
+    steps = sums.shape[0]
+    per_step = count // steps
+    size = tiles * heads
+    row = lax.broadcasted_iota(jnp.int32, (SPAN, SPAN), 0)
+    col = lax.broadcasted_iota(jnp.int32, (SPAN, SPAN), 1)
+    ones = (row // HEAD == col // HEAD).astype(F32).astype(BF16)
+
     def one_step(step, carry):
-        size = tiles * heads
         kept = []
         for place in range(per_step):
             number = step * per_step + place
-            reader, keys, values, decay, learn, scaled = [vectors[w, number] for w in range(6)]
-            direction = scaled / jnp.sqrt(jnp.sum(scaled * scaled, axis=-1, keepdims=True) + 1.0)
+            reader, keys, values, decay, learn = [vectors[w, number] for w in range(5)]
+            direction = directed(number)
             learned = direction * learn
             wide_direction = widen(direction)
             wide_values = widen(values)
             wide_reader = widen(reader * decay)
             base = place * 3 * size
             for i in range(tiles):
-                block = state[number, :, i * span : (i + 1) * span]
-                pick = lane % HEAD == i * copies + lane // HEAD
-                part = slice(base + i * heads, base + (i + 1) * heads)
-                work[part] = (block * wide_direction).astype(BF16)
-                part = slice(base + size + i * heads, base + size + (i + 1) * heads)
-                work[part] = jnp.where(pick, wide_values, 0.0).astype(BF16)
-                product = block * wide_reader
-                high = product.astype(BF16)
-                part = slice(base + 2 * size + i * heads, base + 2 * size + (i + 1) * heads)
-                work[part] = high
+                block = state[number, :, i * SPAN : (i + 1) * SPAN]
+                first = base + i * heads
+                work[first : first + heads] = (block * wide_direction).astype(BF16)
+                first = first + size
+                work[first : first + heads] = jnp.where(pick(i), wide_values, 0.0).astype(BF16)
+                first = first + size
+                work[first : first + heads] = (block * wide_reader).astype(BF16)
             along_learned = jnp.sum(learned * reader, axis=-1, keepdims=True)
             along_keys = jnp.sum(keys * reader, axis=-1, keepdims=True)
-            kept.append(
-                (number, base, widen(decay), widen(learned), widen(keys))
-                + (along_learned, along_keys, values)
-            )
-        sums[...] = dot(work[...], ones)
-        for number, base, wide_decay, wide_learn, wide_keys, along_learned, along_keys, values in kept:
-            picked_removed = jnp.zeros((heads, span), F32)
-            picked_read = jnp.zeros((heads, span), F32)
+            kept.append((number, base, along_learned, along_keys, values))
+        sums[step] = dot(work[...], ones)
+        for number, base, along_learned, along_keys, values in kept:
+            picked_removed = jnp.zeros((heads, SPAN), F32)
+            picked_read = jnp.zeros((heads, SPAN), F32)
             for i in range(tiles):
-                block = state[number, :, i * span : (i + 1) * span]
-                pick = lane % HEAD == i * copies + lane // HEAD
-
-                def summed(which):
-                    first = base + which * size + i * heads
-                    return sums[first : first + heads]
-
-                removed = summed(0)
-                fresh_out[number, :, i * span : (i + 1) * span] = (
-                    block * wide_decay - removed * wide_learn + summed(1) * wide_keys
+                first = base + i * heads
+                picked_removed = jnp.where(
+                    pick(i), sums[step, first : first + heads], picked_removed
                 )
-                picked_removed = jnp.where(pick, removed, picked_removed)
-                picked_read = jnp.where(pick, summed(2), picked_read)
+                first = first + 2 * size
+                picked_read = jnp.where(pick(i), sums[step, first : first + heads], picked_read)
             picked = picked_read - picked_removed * along_learned
             readout = values * along_keys
             for i in range(copies):
@@ -443,9 +386,6 @@
             centre = jnp.mean(readout, axis=-1, keepdims=True)
             spread = jnp.mean(jnp.square(readout - centre), axis=-1, keepdims=True)
             mixed[number] = (readout - centre) * lax.rsqrt(spread + GROUP_EPS)
-        pltpu.make_async_copy(
-            fresh_out.at[rows_of(step)], new_state.at[rows_of(step)], out_sem
-        ).start()
         return carry
 
     lax.fori_loop(0, steps, one_step, 0)
@@ -462,39 +402,35 @@
     token = lax.broadcasted_iota(jnp.int32, (count, count * heads), 0)
     rows = dot((owner == token).astype(F32).astype(BF16), kept).astype(BF16)
     after = (tokens[...].astype(F32) + dot(rows, w_output[...])).astype(BF16)
-    residual[...] = after
-    second[...] = rms_scale(after, second_gain[...]).astype(BF16)
-    pltpu.make_async_copy(fresh_out, new_state, out_sem).wait()
-
-
-def mixer(vectors, state, head_gain, tokens, w_output, second_gain):
-    _, count, heads, _ = vectors.shape
-    width = tokens.shape[1]
-    per_step = 8 if count % 8 == 0 else 1
-    steps = count // per_step
-    rows = per_step * 3 * state.shape[1] * (state.shape[2] // SPAN)
-    vmem = pl.BlockSpec(memory_space=pltpu.VMEM)
-    hbm = pl.BlockSpec(memory_space=pl.ANY)
-    dma = pltpu.SemaphoreType.DMA
-    return pl.pallas_call(
-        functools.partial(mixer_kernel, steps),
-        out_shape=[
-            jax.ShapeDtypeStruct(state.shape, F32),
-            pltpu.VMEM((count, width), BF16),
-            pltpu.VMEM((count, width), BF16),
-        ],
-        in_specs=[vmem] * 6,
-        out_specs=[hbm, vmem, vmem],
-        scratch_shapes=[
-            pltpu.VMEM(state.shape, F32),
-            pltpu.VMEM((count, heads, HEAD), F32),
-            pltpu.VMEM((rows, SPAN), BF16),
-            pltpu.VMEM((rows, SPAN), F32),
-            dma,
-        ],
-        compiler_params=pltpu.CompilerParams(vmem_limit_bytes=VMEM_BYTES),
-        name="mixer",
-    )(vectors, state, head_gain, tokens, w_output, second_gain)
+    return after, rms_scale(after, second_gain[...]).astype(BF16)
+
+
+def mixer_update(vectors, state, sums, new_state):
+    count, heads, tiles, copies, widen, pick, directed = mixer_setup(vectors, state)
+    steps = sums.shape[0]
+    per_step = count // steps
+    size = tiles * heads
+
+    def one_token(number, carry):
+        keys, decay, learn = vectors[1, number], vectors[3, number], vectors[4, number]
+        wide_decay = widen(decay)
+        wide_learn = widen(directed(number) * learn)
+        wide_keys = widen(keys)
+        step = number // per_step
+        base = number % per_step * (3 * size)
+
+        def summed(i, which):
+            first = pl.multiple_of(base + which * size + i * heads, heads)
+            return sums[step, pl.ds(first, heads), :]
+
+        for i in range(tiles):
+            block = state[number, :, i * SPAN : (i + 1) * SPAN]
+            new_state[number, :, i * SPAN : (i + 1) * SPAN] = (
+                block * wide_decay - summed(i, 0) * wide_learn + summed(i, 1) * wide_keys
+            )
+        return carry
+
+    lax.fori_loop(0, count, one_token, 0)
 
 
 def onehot(flags):
@@ -512,66 +448,9 @@
     return first, middle, (rest - middle.astype(F32)).astype(BF16)
 
 
-def experts_kernel(
-    devices,
-    second,
-    residual,
-    routes,
-    route_weights,
-    shared_gate,
-    shared_up,
-    shared_down,
-    expert_gate,
-    expert_up,
-    expert_down,
-    out,
-    sg,
-    su,
-    sd,
-    eg,
-    eu,
-    ed,
-    sbuf,
-    rbuf,
-    pbuf,
-    abuf,
-    local_sem,
-    send_sem,
-    recv_sem,
-):
-    count, width = second.shape
-    total = devices * MOST
-    groups = devices // GROUP
+def plan_routes(devices, routes, route_weights, chosen, pieces_out):
+    total, count = chosen.shape
     me = lax.axis_index("ep")
-    group = me // GROUP
-    place = me % GROUP
-    barrier = pltpu.get_barrier_semaphore()
-    def peers():
-        order = sorted(range(groups), key=lambda g: (-min(g, groups - g), g))
-        for far in order:
-            base = lax.rem(group + far, groups) * GROUP
-            for near in range(GROUP):
-                if far or near:
-                    yield base + lax.rem(place + near, GROUP)
-
-    for peer in peers():
-        pl.semaphore_signal(barrier, inc=1, device_id=(peer,), device_id_type=MESH)
-    loads = [
-        pltpu.make_async_copy(source, target, local_sem.at[number])
-        for number, (source, target) in enumerate(
-            (
-                (shared_gate, sg),
-                (shared_up, su),
-                (shared_down, sd),
-                (expert_gate.at[0], eg),
-                (expert_up.at[0], eu),
-                (expert_down.at[0], ed),
-            )
-        )
-    ]
-    for load in loads:
-        load.start()
-
     lines = lax.broadcasted_iota(jnp.int32, (routes.shape[1], count), 0)
     lanes = lax.broadcasted_iota(jnp.int32, (routes.shape[1], count), 1)
     pick = onehot(lines == me * count + lanes)
@@ -583,10 +462,68 @@
     up_row = lax.broadcasted_iota(jnp.int32, (count, count), 0)
     up_col = lax.broadcasted_iota(jnp.int32, (count, count), 1)
     before = dot(onehot(named), onehot(up_row < up_col))
-    chosen = onehot(named & (before == (line % MOST).astype(F32)))
-    rows = second[...]
-    sbuf[...] = dot(chosen, rows).astype(BF16).reshape(devices, MOST, width)
-    pl.semaphore_wait(barrier, devices - 1)
+    chosen[...] = onehot(named & (before == (line % MOST).astype(F32)))
+    across = lax.broadcasted_iota(jnp.int32, (count, total), 1)
+    named_t = across < 0
+    turned = (((1,), (1,)), ((), ()))
+    lines_t = lax.broadcasted_iota(jnp.int32, (count, routes.shape[1]), 1)
+    lanes_t = lax.broadcasted_iota(jnp.int32, (count, routes.shape[1]), 0)
+    pick_t = onehot(lines_t == me * count + lanes_t)
+
+    def picked(values):
+        return lax.dot_general(pick_t, values, turned, preferred_element_type=F32)
+
+    routes_tall = picked(onehot_values(routes[...]))
+    weights_tall = sum(picked(piece) for piece in thirds(route_weights[...]))
+    weight_t = jnp.zeros((count, total), F32)
+    for j in range(TOPK):
+        hit = routes_tall[:, j : j + 1] == (across // MOST).astype(F32)
+        named_t = named_t | hit
+        weight_t = weight_t + jnp.where(hit, weights_tall[:, j : j + 1], 0.0)
+    before_t = dot(onehot(up_col < up_row), onehot(named_t))
+    weight_t = jnp.where(before_t == (across % MOST).astype(F32), weight_t, 0.0)
+    pieces_out[...] = jnp.concatenate(thirds(weight_t), 0)
+
+
+def experts_kernel(
+    devices,
+    second,
+    residual,
+    chosen,
+    loads,
+    kept_out,
+    abuf,
+    sg,
+    su,
+    sd,
+    eg,
+    eu,
+    ed,
+    sbuf,
+    rbuf,
+    pbuf,
+    send_sem,
+    recv_sem,
+    meet,
+    between,
+):
+    count, width = second.shape
+    total = devices * MOST
+    groups = devices // GROUP
+    me = lax.axis_index("ep")
+    group = me // GROUP
+    place = me % GROUP
+    def peers():
+        order = sorted(range(groups), key=lambda g: (-min(g, groups - g), g))
+        for far in order:
+            base = lax.rem(group + far, groups) * GROUP
+            for near in range(GROUP):
+                if far or near:
+                    yield base + lax.rem(place + near, GROUP)
+
+    rows = second
+    sbuf[...] = dot(chosen[...], rows).astype(BF16).reshape(devices, MOST, width)
+    meet()
 
     def remote(source, target, send, receive, peer):
         return pltpu.make_async_remote_copy(
@@ -622,27 +559,7 @@
     back = (1, pbuf, abuf)
     start_all(*there)
     rbuf[me] = sbuf[me]
-
-    across = lax.broadcasted_iota(jnp.int32, (count, total), 1)
-    named_t = across < 0
-    turned = (((1,), (1,)), ((), ()))
-    lines_t = lax.broadcasted_iota(jnp.int32, (count, routes.shape[1]), 1)
-    lanes_t = lax.broadcasted_iota(jnp.int32, (count, routes.shape[1]), 0)
-    pick_t = onehot(lines_t == me * count + lanes_t)
-
-    def picked(values):
-        return lax.dot_general(pick_t, values, turned, preferred_element_type=F32)
-
-    routes_tall = picked(onehot_values(routes[...]))
-    weights_tall = sum(picked(piece) for piece in thirds(route_weights[...]))
-    weight_t = jnp.zeros((count, total), F32)
-    for j in range(TOPK):
-        hit = routes_tall[:, j : j + 1] == (across // MOST).astype(F32)
-        named_t = named_t | hit
-        weight_t = weight_t + jnp.where(hit, weights_tall[:, j : j + 1], 0.0)
-    before_t = dot(onehot(up_col < up_row), onehot(named_t))
-    weight_t = jnp.where(before_t == (across % MOST).astype(F32), weight_t, 0.0)
-    weight_pieces = jnp.concatenate(thirds(weight_t), 0)
+    between()
 
     def gated(inputs, gate_ref, up_ref):
         gate_part = dot(inputs, gate_ref[...])
@@ -653,7 +570,7 @@
     loads[1].wait()
     shared_hidden = gated(rows, sg, su)
     loads[2].wait()
-    kept = residual[...].astype(F32) + dot(shared_hidden, sd[...])
+    kept_out[...] = residual.astype(F32) + dot(shared_hidden, sd[...])
 
     for load in loads[3:]:
         load.wait()
@@ -663,36 +580,185 @@
     start_all(*back)
     abuf[me] = pbuf[me]
     everything(*back).wait_recv()
-    pieces = dot(weight_pieces, abuf[...].reshape(total, width))
-    routed = pieces[:count] + pieces[count : 2 * count] + pieces[2 * count :]
-    out[...] = (kept + routed).astype(BF16)
     everything(*there).wait_send()
     everything(*back).wait_send()
 
 
-def experts(devices, second, residual, routes, weights, *matrices):
-    count, width = second.shape
+def layer_kernel(devices, refs):
+    (
+        ins,
+        matrices,
+        kept_out,
+        pieces_out,
+        answers,
+        new_state,
+        chosen,
+        vectors,
+        held,
+        project_scratch,
+        mixed,
+        work,
+        sums,
+        expert_scratch,
+        local_sem,
+    ) = refs
+    tokens, state, w_output, head_gain, second_gain, routes, route_weights = held
+    project_kernel(
+        devices,
+        *ins,
+        vectors,
+        *held,
+        *project_scratch,
+        lambda: plan_routes(devices, routes, route_weights, chosen, pieces_out),
+    )
+    me = lax.axis_index("ep")
+    barrier = pltpu.get_barrier_semaphore()
+    for offset in range(1, devices):
+        pl.semaphore_signal(
+            barrier, inc=1, device_id=(lax.rem(me + offset, devices),), device_id_type=MESH
+        )
+    loads = []
+    for number, (source, target) in enumerate(zip(matrices, expert_scratch[:6])):
+        source = source.at[0] if number >= 3 else source
+        loads.append(pltpu.make_async_copy(source, target, local_sem.at[number]))
+        loads[-1].start()
+    residual, second = mixer_read(
+        vectors, state, head_gain, tokens, w_output, second_gain, mixed, work, sums
+    )
+    experts_kernel(
+        devices,
+        second,
+        residual,
+        chosen,
+        loads,
+        kept_out,
+        answers,
+        *expert_scratch,
+        lambda: pl.semaphore_wait(barrier, devices - 1),
+        lambda: mixer_update(vectors, state, sums, new_state),
+    )
+
+
+def layer(devices, smalls, weights, aheads, matrices):
+    tokens, state, w_output = smalls[0], aheads[0], aheads[1]
+    count, width = tokens.shape
+    rows, mix = weights[0].shape
+    heads = mix // HEAD
+    groups = devices // GROUP
+    members = 2 * groups
+    piece = mix // 2 // SPLIT
+    pieces = 3 * SPLIT
+    steps = count // 8 if count % 8 == 0 else 1
+    lines = count // steps * 3 * heads * (state.shape[2] // SPAN)
     vmem = pl.BlockSpec(memory_space=pltpu.VMEM)
     hbm = pl.BlockSpec(memory_space=pltpu.HBM)
     dma = pltpu.SemaphoreType.DMA
     exchange = pltpu.VMEM((devices, MOST, width), BF16)
+    project_scratch = [pltpu.VMEM(array.shape, array.dtype) for array in smalls[1:]] + [
+        pltpu.VMEM((pieces, 2, rows, piece), BF16),
+        pltpu.VMEM((pieces, GROUP * rows, piece), BF16),
+        pltpu.VMEM((groups, count, width // groups), BF16),
+        pltpu.VMEM((members, count, width // groups), BF16),
+        pltpu.VMEM((pieces, members, count, piece), BF16),
+        pltpu.VMEM((pieces, members, count, piece), BF16),
+        dma((len(aheads),)),
+        dma((9,)),
+        dma((3,)),
+        dma,
+        dma((3 * pieces,)),
+        dma,
+        dma,
+        dma,
+        dma((pieces,)),
+    ]
+    expert_scratch = (
+        [pltpu.VMEM(m.shape[-2:], BF16) for m in matrices] + [exchange] * 3 + [dma((2,))] * 2
+    )
+    held = [pltpu.VMEM(array.shape, array.dtype) for array in (tokens,) + aheads]
+    shapes = [
+        [None] * (len(smalls) + len(weights) + len(aheads)),
+        [None] * len(matrices),
+        None,
+        None,
+        None,
+        None,
+        pltpu.VMEM((devices * MOST, count), BF16),
+        pltpu.VMEM((6, count, heads, HEAD), F32),
+        held,
+        project_scratch,
+        pltpu.VMEM((count, heads, HEAD), F32),
+        pltpu.VMEM((lines, SPAN), BF16),
+        pltpu.VMEM((steps, lines, SPAN), F32),
+        expert_scratch,
+        dma((len(matrices),)),
+    ]
+
+    def kernel(*flat):
+        rest = iter(flat)
+        layer_kernel(
+            devices,
+            [[next(rest) for _ in s] if isinstance(s, list) else next(rest) for s in shapes],
+        )
+
+    scratch = []
+    for shape in shapes[6:]:
+        scratch.extend(shape if isinstance(shape, list) else [shape])
+    operands = (*smalls, *weights, *aheads, *matrices)
     return pl.pallas_call(
-        functools.partial(experts_kernel, devices),
-        out_shape=pltpu.VMEM((count, width), BF16),
-        in_specs=[vmem] * 4 + [hbm] * 6,
-        out_specs=vmem,
-        scratch_shapes=[pltpu.VMEM(m.shape[-2:], BF16) for m in matrices]
-        + [exchange] * 4
-        + [
-            dma((6,)),
-            dma((2,)),
-            dma((2,)),
+        kernel,
+        out_shape=[
+            pltpu.VMEM((count, width), F32),
+            pltpu.VMEM((3 * count, devices * MOST), BF16),
+            exchange,
+            pltpu.VMEM(state.shape, F32),
         ],
+        in_specs=[hbm] * len(operands),
+        out_specs=[vmem] * 4,
+        scratch_shapes=scratch,
         compiler_params=pltpu.CompilerParams(
-            collective_id=1, has_side_effects=True, vmem_limit_bytes=VMEM_BYTES
+            collective_id=0, has_side_effects=True, vmem_limit_bytes=VMEM_BYTES
         ),
-        name="experts",
-    )(second, residual, routes, weights, *map(pinned, matrices))
+        name="layer",
+    )(*map(pinned, operands))
+
+
+def close_kernel(kept, weight_pieces, answers, state, out, new_state, mixed, sem, out_sem):
+    count = kept.shape[0]
+    chunks = sem.shape[0]
+    copies = []
+    for number in range(chunks):
+        span = pl.ds(number * (count // chunks), count // chunks)
+        copies.append(pltpu.make_async_copy(state.at[span], new_state.at[span], sem.at[number]))
+        copies[-1].start()
+    total = weight_pieces.shape[1]
+    pieces = dot(weight_pieces[...], answers[...].reshape(total, kept.shape[1]))
+    routed = pieces[:count] + pieces[count : 2 * count] + pieces[2 * count :]
+    mixed[...] = (kept[...] + routed).astype(BF16)
+    copies.append(pltpu.make_async_copy(mixed, out, out_sem))
+    copies[-1].start()
+    for copy in copies:
+        copy.wait()
+
+
+def close(kept, weight_pieces, answers, state):
+    vmem = pl.BlockSpec(memory_space=pltpu.VMEM)
+    hbm = pl.BlockSpec(memory_space=pltpu.HBM)
+    return pl.pallas_call(
+        close_kernel,
+        out_shape=[
+            jax.ShapeDtypeStruct(kept.shape, BF16),
+            jax.ShapeDtypeStruct(state.shape, F32),
+        ],
+        in_specs=[vmem] * 4,
+        out_specs=[hbm, hbm],
+        scratch_shapes=[
+            pltpu.VMEM(kept.shape, BF16),
+            pltpu.SemaphoreType.DMA((8 if state.shape[0] % 8 == 0 else 1,)),
+            pltpu.SemaphoreType.DMA,
+        ],
+        compiler_params=pltpu.CompilerParams(vmem_limit_bytes=CLOSE_BYTES),
+        name="close",
+    )(kept, weight_pieces, answers, state)
 
 
 def pinned(array):
@@ -726,8 +792,19 @@
     route_weights,
 ):
     devices = lax.axis_size("ep")
-    vectors, *ahead = project(
+    results = layer(
         devices,
+        (
+            tokens,
+            first_gain[None, :],
+            decay_down.T,
+            decay_up,
+            decay_base[None, :],
+            rate_down.T,
+            rate_up,
+            rate_base[None, :],
+            key_scale[None, :],
+        ),
         (w_receptance, w_key, w_value),
         (
             recurrent_state,
@@ -737,32 +814,9 @@
             routes.T,
             route_weights.T,
         ),
-        tokens,
-        first_gain[None, :],
-        decay_down.T,
-        decay_up,
-        decay_base[None, :],
-        rate_down.T,
-        rate_up,
-        rate_base[None, :],
-        key_scale[None, :],
+        (shared_gate, shared_up, shared_down, expert_gate, expert_up, expert_down),
     )
-    tokens, state, w_output, head_gain, second_gain, routes, route_weights = ahead
-    new_state, residual, second = mixer(vectors, state, head_gain, tokens, w_output, second_gain)
-    new_tokens = experts(
-        devices,
-        second,
-        residual,
-        routes,
-        route_weights,
-        shared_gate,
-        shared_up,
-        shared_down,
-        expert_gate,
-        expert_up,
-        expert_down,
-    )
-    return (new_tokens, new_state)
+    return close(*results)
 
 
 def solution(mesh):

time: 61.7 us -> 59.9 us (0.971)
  Pallas kernels: 60.1 us -> 59 us
  local copies, waits for them, and re-layouts: 0.63 us -> 0 us
    pallas_call x3 -> x2, Pallas kernels: 60.1 us -> 59 us  [the longest x1 56.9 us: layer(): pl.pallas_call(kernel, out_shape=[pltpu.VMEM((count, width), F32), pltpu....]
    unnamed x1 -> x0, local copies, waits for them, and re-layouts: 0.63 us -> none
where the time goes in v4:
time: 59.9 us; the launch traced here: 59.6 us
  Pallas kernels  59 us (98%)
  between operations  0.65 us (1%)
    pallas_call x1, Pallas kernels, layer(): pl.pallas_call(kernel, out_shape=[pltpu.VMEM((count, width), F32), pltpu....  56.9 us
    pallas_call x1, Pallas kernels, close(): pl.pallas_call(close_kernel, out_shape=[jax.ShapeDtypeStruct(kept.shape,...  2.09 us

profile of v4, /device:TPU:0, one launch (start us, length us, event | category | flops | bytes accessed | tf_op | source)
XLA Modules:
  0.0 59.6 jit_solution(1084263371561243435)
XLA Ops:
  0.6 56.9 %layer.1 = (f32[16,2048]{1,0:T(8,128)S(1)}, bf16[48,128]{1,0:T(8,128)(2,1)S(1)}, bf16[32,4,2048]{2,1,0:T(4,128)(2,1)S(1)}, f32[16,16,4096]{2,1,0:T(8,128)S(1)}) custom-call(bf16[16,2048]{1,0:T(8,128)(2,1)} %flat_0_.1, f32[1,2048]{1,0:T(1,128)} %bitcast.12, bf16[64,2048]{1,0:T(8,128)(2,1)} %bitcast.10, bf16[64,1024]{1,0:T(8,128)(2,1)} %flat_3_.1, ...), custom_call_target="tpu_custom_call" | custom-call | tf_op jit(solution)/shard_map/layer/pallas_call | solution.py:707
  57.5 2.1 %close.1 = (bf16[16,2048]{1,0:T(8,128)(2,1)}, f32[16,16,4096]{2,1,0:T(8,128)}) custom-call(f32[16,2048]{1,0:T(8,128)S(1)} %get-tuple-element.6.kept, bf16[48,128]{1,0:T(8,128)(2,1)S(1)} %get-tuple-element.7.weight_pieces, bf16[32,4,2048]{2,1,0:T(4,128)(2,1)S(1)} %get-tuple-element.8.answers, f32[16,16,4096]{2,1,0:T(8,128)S(1)} %get-tuple-element.9.state), custom_call_target="tpu_custom_call" | custom-call | tf_op jit(solution)/shard_map/close/pallas_call | solution.py:746

commit v5 on v4

--- a/solution.py
+++ b/solution.py
@@ -516,7 +516,8 @@
     def peers():
         order = sorted(range(groups), key=lambda g: (-min(g, groups - g), g))
         for far in order:
-            base = lax.rem(group + far, groups) * GROUP
+            turned = far + (1 - group % 2) * (groups - 2 * far) if far else far
+            base = lax.rem(group + turned, groups) * GROUP
             for near in range(GROUP):
                 if far or near:
                     yield base + lax.rem(place + near, GROUP)

time: 59.9 us -> 59.8 us (level)
  no operation moved by 1% of the time
where the time goes in v5:
time: 59.8 us; the launch traced here: 59.6 us
  Pallas kernels  59 us (99%)
  between operations  0.65 us (1%)
    pallas_call x1, Pallas kernels, layer(): pl.pallas_call(kernel, out_shape=[pltpu.VMEM((count, width), F32), pltpu....  56.9 us
    pallas_call x1, Pallas kernels, close(): pl.pallas_call(close_kernel, out_shape=[jax.ShapeDtypeStruct(kept.shape,...  2.09 us

profile of v5, /device:TPU:0, one launch (start us, length us, event | category | flops | bytes accessed | tf_op | source)
XLA Modules:
  0.0 59.6 jit_solution(11971949374467602190)
XLA Ops:
  0.6 56.9 %layer.1 = (f32[16,2048]{1,0:T(8,128)S(1)}, bf16[48,128]{1,0:T(8,128)(2,1)S(1)}, bf16[32,4,2048]{2,1,0:T(4,128)(2,1)S(1)}, f32[16,16,4096]{2,1,0:T(8,128)S(1)}) custom-call(bf16[16,2048]{1,0:T(8,128)(2,1)} %flat_0_.1, f32[1,2048]{1,0:T(1,128)} %bitcast.12, bf16[64,2048]{1,0:T(8,128)(2,1)} %bitcast.10, bf16[64,1024]{1,0:T(8,128)(2,1)} %flat_3_.1, ...), custom_call_target="tpu_custom_call" | custom-call | tf_op jit(solution)/shard_map/layer/pallas_call | solution.py:708
  57.5 2.1 %close.1 = (bf16[16,2048]{1,0:T(8,128)(2,1)}, f32[16,16,4096]{2,1,0:T(8,128)}) custom-call(f32[16,2048]{1,0:T(8,128)S(1)} %get-tuple-element.6.kept, bf16[48,128]{1,0:T(8,128)(2,1)S(1)} %get-tuple-element.7.weight_pieces, bf16[32,4,2048]{2,1,0:T(4,128)(2,1)S(1)} %get-tuple-element.8.answers, f32[16,16,4096]{2,1,0:T(8,128)S(1)} %get-tuple-element.9.state), custom_call_target="tpu_custom_call" | custom-call | tf_op jit(solution)/shard_map/close/pallas_call | solution.py:747
